TPU v7x, 32 devices: a whole 2x2x4 slice. The times are simulated.
32 devices in a mesh: sp: 4 (over z), tp: 4 (over y, x), dp: 2 (over core).
Axes of the slice: x: 2, y: 2, z: 4, core: 2. Of those that a mesh axis runs over, the one named last changes fastest.
Arguments:
- latent: bfloat16 [4, 4096, 2048], P('dp', 'sp'), may hold values from -6 to 6
- context: bfloat16 [4, 1024, 2048], P('dp', 'sp'), may hold values from -6 to 6
- condition: bfloat16 [4, 2048], P('dp', 'sp'), may hold values from -6 to 6
- ctx_cond: bfloat16 [2048], P('sp'), may hold values from -6 to 6
- norm_gain: float32 [2048], replicated, may hold values from 0.1 to 1.9
- w_shift: bfloat16 [2048, 2048], P('sp', 'tp'), may hold values from -0.125 to 0.125
- w_scale: bfloat16 [2048, 2048], P('sp', 'tp'), may hold values from -0.125 to 0.125
- w_gate: bfloat16 [2048, 2048], P('sp', 'tp'), may hold values from -0.125 to 0.125
- w_query: bfloat16 [2048, 1024], P(None, 'tp'), may hold values from -0.125 to 0.125
- w_key: bfloat16 [2048, 256], P(None, 'tp'), may hold values from -0.125 to 0.125
- w_value: bfloat16 [2048, 256], P(None, 'tp'), may hold values from -0.125 to 0.125
- w_out: bfloat16 [1024, 2048], P('tp'), may hold values from -4 to 4
- sink_logit: float32 [16], P('tp'), may hold values from 4 to 7
- ctx_lift: float32 [16], P('tp'), may hold values from -4 to 220
Outputs:
- mixed: bfloat16 [4, 4096, 2048], P('dp', ('sp', 'tp'))
All inputs are finite; a program needn't handle non-finite values.
Results may differ from a plain program's by a relative error of at most 0.012.
Values may be sent and summed in bfloat16 or wider, within the bound.
No kernel may reach another device: no remote copies, remote signals or barrier semaphores. Data moves between devices by JAX's collectives and lax.ppermute only.
A program may use at most 128 MiB of HBM per device.

v0:
```python
import jax
import jax.numpy as jnp
from jax import lax
from jax.sharding import PartitionSpec as P

HEAD = 64
WINDOW = 128
GRID_COLS = 64


epsilon = 1e-06
rope_base = 10000.0
masked_value = -1e30


def with_halo(cells, sides, width):
    for axis, dim in sides:
        count = lax.axis_size(axis)
        ends = count - 1
        head = lax.slice_in_dim(cells, 0, width, axis=dim)
        tail = lax.slice_in_dim(cells, cells.shape[dim] - width, cells.shape[dim], axis=dim)
        cells = jnp.concatenate(
            [
                lax.ppermute(tail, axis, [(i, (i + 1) % count) for i in range(ends)]),
                cells,
                lax.ppermute(head, axis, [((i + 1) % count, i) for i in range(ends)]),
            ],
            axis=dim,
        )
    return cells


def modulated(inputs, norm_gain, shift_vec, scale_vec):
    widened = inputs.astype(jnp.float32)
    inverse = lax.rsqrt(jnp.mean(widened * widened, axis=-1, keepdims=True) + epsilon)
    return (widened * inverse * norm_gain * (1.0 + scale_vec) + shift_vec).astype(jnp.bfloat16)


def rotate_half(half_part, angles):
    first_half, second = jnp.split(half_part, 2, axis=-1)
    cosine = jnp.cos(angles)[:, None, :]
    sine_part = jnp.sin(angles)[:, None, :]
    return jnp.concatenate(
        [first_half * cosine - second * sine_part, first_half * sine_part + second * cosine],
        axis=-1,
    )


def rotate(inputs, positions):
    quarter = inputs.shape[-1] // 4
    frequency = rope_base ** (-jnp.arange(quarter, dtype=jnp.float32) / quarter)
    row_angle = (positions // GRID_COLS).astype(jnp.float32)[:, None] * frequency
    col_angle = (positions % GRID_COLS).astype(jnp.float32)[:, None] * frequency
    half_size = 2 * quarter
    return jnp.concatenate(
        [
            rotate_half(inputs[..., :half_size], row_angle),
            rotate_half(inputs[..., half_size:], col_angle),
        ],
        axis=-1,
    )


def shards(
    latent,
    context,
    condition,
    ctx_cond,
    norm_gain,
    w_shift,
    w_scale,
    w_gate,
    w_query,
    w_key,
    w_value,
    w_out,
    sink_logit,
    ctx_lift,
):
    samples, tokens, model_width = latent.shape
    head_size = HEAD
    sp_count = lax.axis_size("sp")
    cond_rows = jnp.concatenate([condition, ctx_cond[None, :]], axis=0)
    active = jax.nn.silu(cond_rows.astype(jnp.float32)).astype(jnp.bfloat16)
    shift_part, scale_part, gate_part = lax.psum(
        (
            jnp.dot(active, w_shift, preferred_element_type=jnp.float32),
            jnp.dot(active, w_scale, preferred_element_type=jnp.float32),
            jnp.dot(active, w_gate, preferred_element_type=jnp.float32),
        ),
        "sp",
    )
    shift_vec, scale_vec, gate_vec = (
        lax.all_gather(shift_part, "tp", axis=1, tiled=True),
        lax.all_gather(scale_part, "tp", axis=1, tiled=True),
        lax.all_gather(gate_part, "tp", axis=1, tiled=True),
    )
    hidden = modulated(
        latent, norm_gain, shift_vec[:samples, None, :], scale_vec[:samples, None, :]
    )
    offset_row = lax.axis_index("sp") * tokens
    positions = offset_row + jnp.arange(tokens, dtype=jnp.int32)
    query_heads = w_query.shape[1] // head_size
    key_heads = w_key.shape[1] // head_size
    group_size = query_heads // key_heads
    keyed = key_heads * head_size
    queries = rotate(
        jnp.einsum("snd,dc->snc", hidden, w_query, preferred_element_type=jnp.float32).reshape(
            samples, tokens, query_heads, head_size
        ),
        positions,
    ).astype(jnp.bfloat16)
    key_rows = rotate(
        jnp.einsum("snd,dc->snc", hidden, w_key, preferred_element_type=jnp.float32).reshape(
            samples, tokens, key_heads, head_size
        ),
        positions,
    ).astype(jnp.bfloat16)
    values = jnp.einsum("snd,dc->snc", hidden, w_value, preferred_element_type=jnp.float32).astype(
        jnp.bfloat16
    )
    local_pairs = jnp.concatenate([key_rows.reshape(samples, tokens, keyed), values], axis=-1)
    extended = with_halo(local_pairs, (("sp", 1),), WINDOW)
    ctx_hidden = modulated(context, norm_gain, shift_vec[samples], scale_vec[samples])
    ctx_keys = jnp.einsum(
        "snd,dc->snc", ctx_hidden, w_key, preferred_element_type=jnp.float32
    ).astype(jnp.bfloat16)
    ctx_values = jnp.einsum(
        "snd,dc->snc", ctx_hidden, w_value, preferred_element_type=jnp.float32
    ).astype(jnp.bfloat16)
    context_pairs = lax.all_gather(
        jnp.concatenate([ctx_keys, ctx_values], axis=-1), "sp", axis=1, tiled=True
    )
    block_rows = min(512, tokens)
    blocks = tokens // block_rows
    span_rows = block_rows + 2 * WINDOW
    latent_len = tokens * sp_count
    lift_rows = ctx_lift.reshape(key_heads, group_size, 1, 1)
    sink_rows = sink_logit.reshape(key_heads, group_size, 1, 1)
    factor = head_size ** (-0.5)

    def attend(step_id):
        sample = step_id // blocks
        row_start = step_id % blocks * block_rows
        q_rows = lax.dynamic_slice_in_dim(
            lax.dynamic_index_in_dim(queries, sample, 0, keepdims=False), row_start, block_rows, 0
        )
        q_rows = q_rows.reshape(block_rows, key_heads, group_size, head_size)
        pair_rows = lax.dynamic_slice_in_dim(
            lax.dynamic_index_in_dim(extended, sample, 0, keepdims=False), row_start, span_rows, 0
        )
        near_keys = pair_rows[:, :keyed].reshape(span_rows, key_heads, head_size)
        near_values = pair_rows[:, keyed:].reshape(span_rows, key_heads, head_size)
        ctx_rows = lax.dynamic_index_in_dim(context_pairs, sample, 0, keepdims=False)
        far_keys = ctx_rows[:, :keyed].reshape(-1, key_heads, head_size)
        far_values = ctx_rows[:, keyed:].reshape(-1, key_heads, head_size)
        query_pos = offset_row + row_start + jnp.arange(block_rows, dtype=jnp.int32)
        key_pos = offset_row + row_start - WINDOW + jnp.arange(span_rows, dtype=jnp.int32)
        inside = (
            (key_pos[None, :] >= 0)
            & (key_pos[None, :] < latent_len)
            & (jnp.abs(query_pos[:, None] - key_pos[None, :]) <= WINDOW)
        )
        near_scores = (
            jnp.einsum("qgrd,kgd->grqk", q_rows, near_keys, preferred_element_type=jnp.float32)
            * factor
        )
        near_scores = jnp.where(inside[None, None], near_scores, masked_value)
        far_scores = (
            jnp.einsum("qgrd,kgd->grqk", q_rows, far_keys, preferred_element_type=jnp.float32)
            * factor
            + lift_rows
        )
        row_max = jnp.maximum(
            jnp.maximum(near_scores.max(-1, keepdims=True), far_scores.max(-1, keepdims=True)),
            sink_rows,
        )
        near_exp = jnp.exp(near_scores - row_max)
        far_exp = jnp.exp(far_scores - row_max)
        normaliser = (
            near_exp.sum(-1, keepdims=True)
            + far_exp.sum(-1, keepdims=True)
            + jnp.exp(sink_rows - row_max)
        )
        outcome = jnp.einsum(
            "grqk,kgd->qgrd",
            (near_exp / normaliser).astype(jnp.bfloat16),
            near_values,
            preferred_element_type=jnp.float32,
        )
        outcome = outcome + jnp.einsum(
            "grqk,kgd->qgrd",
            (far_exp / normaliser).astype(jnp.bfloat16),
            far_values,
            preferred_element_type=jnp.float32,
        )
        return outcome.astype(jnp.bfloat16).reshape(block_rows, query_heads * head_size)

    attended = lax.map(attend, jnp.arange(samples * blocks, dtype=jnp.int32)).reshape(
        samples, tokens, query_heads * head_size
    )
    by_rows = lax.all_to_all(attended, "tp", split_axis=1, concat_axis=2, tiled=True)
    projected = jnp.einsum(
        "snc,cd->snd",
        by_rows,
        lax.all_gather(w_out, "tp", axis=0, tiled=True),
        preferred_element_type=jnp.float32,
    )
    return (gate_vec[:samples, None, :] * projected).astype(jnp.bfloat16)


def solution(mesh):
    return jax.shard_map(
        shards,
        mesh=mesh,
        in_specs=(
            P("dp", "sp", None),
            P("dp", "sp", None),
            P("dp", "sp"),
            P("sp"),
            P(),
            P("sp", "tp"),
            P("sp", "tp"),
            P("sp", "tp"),
            P(None, "tp"),
            P(None, "tp"),
            P(None, "tp"),
            P("tp", None),
            P("tp"),
            P("tp"),
        ),
        out_specs=P("dp", ("sp", "tp"), None),
        check_vma=False,
    )
```

profile of v0, /device:TPU:0, one launch (start us, length us, event | category | flops | bytes accessed | tf_op | source)
XLA Modules:
  0.0 226.5 jit_solution(14336475768110559586)
XLA Ops:
  11.1 21.3 %all-reduce = (f32[3,512]{1,0:T(4,128)S(1)}, f32[3,512]{1,0:T(4,128)S(1)}, f32[3,512]{1,0:T(4,128)}) all-reduce(f32[3,512]{1,0:T(4,128)S(1)} %fusion.70, f32[3,512]{1,0:T(4,128)S(1)} %fusion.72, f32[3,512]{1,0:T(4,128)S(1)} %fusion.74), channel_id=1, replica_groups=mesh['sp'=4,'tp'=4,'dp'=2] {'sp'}, use_global_device_ids=true, to_apply=%region_3.4 | all-reduce | flops 4608 | bytes 36864 | tf_op jit(solution)/shard_map/psum | solution.py:85
  32.3 8.2 %all_gather.17 = f32[3,2048]{1,0:T(4,128)S(1)} all-gather(f32[3,512]{1,0:T(4,128)S(1)} %get-tuple-element.178), channel_id=1, replica_groups=mesh['sp'=4,'tp'=4,'dp'=2] {'tp'}, dimensions={1}, use_global_device_ids=true | all-gather | bytes 30720 | tf_op jit(solution)/shard_map/all_gather | solution.py:94
  40.5 8.2 %all_gather.16 = f32[3,2048]{1,0:T(4,128)S(1)} all-gather(f32[3,512]{1,0:T(4,128)S(1)} %get-tuple-element.179), channel_id=1, replica_groups=mesh['sp'=4,'tp'=4,'dp'=2] {'tp'}, dimensions={1}, use_global_device_ids=true | all-gather | bytes 30720 | tf_op jit(solution)/shard_map/all_gather | solution.py:95
  48.7 5.1 %fusion.26 = f32[2,1024]{1,0:T(2,128)S(1)} fusion(bf16[2,1024,2048]{2,1,0:T(8,128)(2,1)} %param.16), kind=kLoop, calls=%fused_computation.44 | loop fusion | flops 12580864 | bytes 8396800 | tf_op jit(solution)/shard_map/reduce_sum | solution.py:35
  54.4 6.0 %convolution_bitcast_fusion = f32[2,1024,1,64]{1,3,0,2:T(8,128)S(1)} fusion(bf16[2,1024,2048]{2,1,0:T(8,128)(2,1)} %param.16, f32[2,2048]{1,0:T(2,128)S(1)} %slice.74, f32[2,2048]{1,0:T(2,128)S(1)} %slice_add_fusion, f32[2048]{0:T(1024)S(1)} %copy-done.6, f32[2,1024]{1,0:T(2,128)S(1)} %add_rsqrt_fusion, bf16[2048,64]{0,1:T(8,128)(2,1)S(1)} %copy-done.5), kind=kOutput, calls=%fused_computation.59 | convolution fusion | flops 562036736 | bytes 9224192 | tf_op jit(solution)/shard_map/snd,dc->snc/dot_general | solution.py:114
  60.5 6.9 %fusion.40 = bf16[2,1024,128]{1,2,0:T(8,128)(2,1)S(1)} fusion(bf16[2,1024,128]{1,2,0:T(8,128)(2,1)S(1)} %fusion.59, bf16[2,1024,2048]{2,1,0:T(8,128)(2,1)} %param.16, f32[2,2048]{1,0:T(2,128)S(1)} %slice.74, f32[2,2048]{1,0:T(2,128)S(1)} %slice_add_fusion, f32[2048]{0:T(1024)S(1)} %copy-done.6, f32[2,1024]{1,0:T(2,128)S(1)} %add_rsqrt_fusion, ...), kind=kOutput, calls=%fused_computation.61 | convolution fusion | flops 562167808 | bytes 8962048 | tf_op jit(solution)/shard_map/snd,dc->snc/dot_general | solution.py:119
  72.4 2.6 %convolution_convert_fusion.1 = bf16[2,256,64]{1,2,0:T(8,128)(2,1)S(1)} fusion(bf16[2,256,2048]{2,1,0:T(8,128)(2,1)} %param.17, f32[2048]{0:T(1024)S(1)} %bitcast.202, f32[2048]{0:T(1024)S(1)} %bitcast.200, f32[2048]{0:T(1024)S(1)} %copy-done.6, f32[2,256]{1,0:T(2,128)S(1)} %add_rsqrt_fusion.1, bf16[2048,64]{0,1:T(8,128)(2,1)S(1)} %copy-done.4), kind=kOutput, calls=%fused_computation.62 | convolution fusion | flops 140541952 | bytes 2451456 | tf_op jit(solution)/shard_map/snd,dc->snc/dot_general | solution.py:128
  75.1 2.6 %convolution_convert_fusion.2 = bf16[2,256,64]{1,2,0:T(8,128)(2,1)S(1)} fusion(bf16[2,256,2048]{2,1,0:T(8,128)(2,1)} %param.17, f32[2048]{0:T(1024)S(1)} %bitcast.203, f32[2048]{0:T(1024)S(1)} %bitcast.201, f32[2048]{0:T(1024)S(1)} %copy-done.6, f32[2,256]{1,0:T(2,128)S(1)} %add_rsqrt_fusion.1, bf16[2048,64]{0,1:T(8,128)(2,1)S(1)} %copy-done.5), kind=kOutput, calls=%fused_computation.63 | convolution fusion | flops 140541952 | bytes 2451456 | tf_op jit(solution)/shard_map/snd,dc->snc/dot_general | solution.py:125
  77.7 6.7 %fusion.43 = f32[2,1024,256]{1,2,0:T(8,128)S(1)} fusion(bf16[2048,256]{1,0:T(8,128)(2,1)S(1)} %copy-done, bf16[2,1024,2048]{2,1,0:T(8,128)(2,1)} %param.16, f32[2,2048]{1,0:T(2,128)S(1)} %slice.74, f32[2,2048]{1,0:T(2,128)S(1)} %slice_add_fusion, f32[2048]{0:T(1024)S(1)} %copy-done.6, f32[2,1024]{1,0:T(2,128)S(1)} %add_rsqrt_fusion), kind=kOutput, calls=%fused_computation.65 | convolution fusion | flops 2172649472 | bytes 11583488 | tf_op jit(solution)/shard_map/snd,dc->snc/dot_general | solution.py:108
  84.8 15.8 %all_gather.18 = bf16[2,1024,128]{1,2,0:T(8,128)(2,1)S(1)} all-gather(bf16[2,256,128]{1,2,0:T(8,128)(2,1)S(1)} %pad_maximum_fusion.2), channel_id=1, replica_groups=mesh['sp'=4,'tp'=4,'dp'=2] {'sp'}, dimensions={1}, use_global_device_ids=true | all-gather | bytes 655360 | tf_op jit(solution)/shard_map/all_gather | solution.py:131
  102.2 91.8 %while.13 = (s32[]{:T(128)}, bf16[4,512,256]{2,1,0:T(8,128)(2,1)}, s32[4]{0:T(128)}, bf16[2,1280,128]{1,2,0:T(8,128)(2,1)}, s32[]{:T(128)}, /*index=5*/bf16[2,10...) while((s32[]{:T(128)}, bf16[4,512,256]{2,1,0:T(8,128)(2,1)}, ...), condition=%wide.region_10.11_spmd, body=%wide.region_5.10_spmd.sunk | while | flops 985405696 | bytes 75191968 | solution.py:199
  105.8 4.6 %bitcast_reduce_fusion.2 = (f32[4,512]{1,0:T(4,128)S(1)}, f32[1024,512,4]{1,0,2:T(8,128)}) fusion(f32[4]{0:T(128)S(1)} %bitcast.194, bf16[2,1024,4,64]{1,3,2,0:T(8,128)(2,1)S(1)} %get-tuple-element.303, s32[]{:T(128)S(6)} %select_n.121, s32[]{:T(128)S(6)} %select_n.124, bf16[1024,128]{0,1:T(8,128)(2,1)S(1)} %dynamic-slice_bitcast_fusion.4), kind=kOutput, calls=%fused_computation.1.clone.1 | convolution fusion | flops 274724864 | bytes 8790536 | tf_op jit(solution)/shard_map/while/body/eval_jaxpr/qgrd,kgd->grqk/dot_general | solution.py:170
  113.4 5.2 %fusion.94 = f32[4,512]{1,0:T(4,128)S(1)} fusion(f32[1024,512,4]{1,0,2:T(8,128)} %get-tuple-element.260, f32[4,512]{1,0:T(4,128)S(1)} %maximum_maximum_fusion.2, f32[4]{0:T(128)S(1)} %bitcast.195), kind=kLoop, calls=%fused_computation.5.clone.1 | loop fusion | flops 8386560 | bytes 8405008 | tf_op jit(solution)/shard_map/while/body/eval_jaxpr/reduce_sum | solution.py:182
  120.2 2.1 fusion.95
  128.8 4.6 %bitcast_reduce_fusion.2 = (f32[4,512]{1,0:T(4,128)S(1)}, f32[1024,512,4]{1,0,2:T(8,128)}) fusion(f32[4]{0:T(128)S(1)} %bitcast.194, bf16[2,1024,4,64]{1,3,2,0:T(8,128)(2,1)S(1)} %get-tuple-element.303, s32[]{:T(128)S(6)} %select_n.121, s32[]{:T(128)S(6)} %select_n.124, bf16[1024,128]{0,1:T(8,128)(2,1)S(1)} %dynamic-slice_bitcast_fusion.4), kind=kOutput, calls=%fused_computation.1.clone.1 | convolution fusion | flops 274724864 | bytes 8790536 | tf_op jit(solution)/shard_map/while/body/eval_jaxpr/qgrd,kgd->grqk/dot_general | solution.py:170
  136.4 5.2 %fusion.94 = f32[4,512]{1,0:T(4,128)S(1)} fusion(f32[1024,512,4]{1,0,2:T(8,128)} %get-tuple-element.260, f32[4,512]{1,0:T(4,128)S(1)} %maximum_maximum_fusion.2, f32[4]{0:T(128)S(1)} %bitcast.195), kind=kLoop, calls=%fused_computation.5.clone.1 | loop fusion | flops 8386560 | bytes 8405008 | tf_op jit(solution)/shard_map/while/body/eval_jaxpr/reduce_sum | solution.py:182
  151.7 4.6 %bitcast_reduce_fusion.2 = (f32[4,512]{1,0:T(4,128)S(1)}, f32[1024,512,4]{1,0,2:T(8,128)}) fusion(f32[4]{0:T(128)S(1)} %bitcast.194, bf16[2,1024,4,64]{1,3,2,0:T(8,128)(2,1)S(1)} %get-tuple-element.303, s32[]{:T(128)S(6)} %select_n.121, s32[]{:T(128)S(6)} %select_n.124, bf16[1024,128]{0,1:T(8,128)(2,1)S(1)} %dynamic-slice_bitcast_fusion.4), kind=kOutput, calls=%fused_computation.1.clone.1 | convolution fusion | flops 274724864 | bytes 8790536 | tf_op jit(solution)/shard_map/while/body/eval_jaxpr/qgrd,kgd->grqk/dot_general | solution.py:170
  159.3 5.2 %fusion.94 = f32[4,512]{1,0:T(4,128)S(1)} fusion(f32[1024,512,4]{1,0,2:T(8,128)} %get-tuple-element.260, f32[4,512]{1,0:T(4,128)S(1)} %maximum_maximum_fusion.2, f32[4]{0:T(128)S(1)} %bitcast.195), kind=kLoop, calls=%fused_computation.5.clone.1 | loop fusion | flops 8386560 | bytes 8405008 | tf_op jit(solution)/shard_map/while/body/eval_jaxpr/reduce_sum | solution.py:182
  174.6 4.6 %bitcast_reduce_fusion.2 = (f32[4,512]{1,0:T(4,128)S(1)}, f32[1024,512,4]{1,0,2:T(8,128)}) fusion(f32[4]{0:T(128)S(1)} %bitcast.194, bf16[2,1024,4,64]{1,3,2,0:T(8,128)(2,1)S(1)} %get-tuple-element.303, s32[]{:T(128)S(6)} %select_n.121, s32[]{:T(128)S(6)} %select_n.124, bf16[1024,128]{0,1:T(8,128)(2,1)S(1)} %dynamic-slice_bitcast_fusion.4), kind=kOutput, calls=%fused_computation.1.clone.1 | convolution fusion | flops 274724864 | bytes 8790536 | tf_op jit(solution)/shard_map/while/body/eval_jaxpr/qgrd,kgd->grqk/dot_general | solution.py:170
  182.2 5.2 %fusion.94 = f32[4,512]{1,0:T(4,128)S(1)} fusion(f32[1024,512,4]{1,0,2:T(8,128)} %get-tuple-element.260, f32[4,512]{1,0:T(4,128)S(1)} %maximum_maximum_fusion.2, f32[4]{0:T(128)S(1)} %bitcast.195), kind=kLoop, calls=%fused_computation.5.clone.1 | loop fusion | flops 8386560 | bytes 8405008 | tf_op jit(solution)/shard_map/while/body/eval_jaxpr/reduce_sum | solution.py:182
  194.0 3.3 %copy.27 = bf16[2,1024,256]{2,0,1:T(2,128)(2,1)} copy(bf16[2,1024,256]{2,1,0:T(8,128)(2,1)} %bitcast.191) | data formatting | bytes 2097152 | tf_op jit(solution)/shard_map/reshape | solution.py:199
  197.3 3.5 %all-to-all-start = ((bf16[2,1024,256]{2,0,1:T(2,128)(2,1)}), bf16[2,1024,256]{2,0,1:T(2,128)(2,1)S(1)}, u32[]{:S(2)}, u32[]{:S(2)}) async-start(bf16[2,1024,256]{2,0,1:T(2,128)(2,1)} %copy.27), calls=%async_computation | async-start | bytes 2097152 | tf_op jit(solution)/shard_map/all_to_all | solution.py:202
  200.8 12.7 %all_gather.15 = f32[3,2048]{1,0:T(4,128)S(1)} all-gather(f32[3,512]{1,0:T(4,128)S(1)} %copy-done.3), channel_id=1, replica_groups=mesh['sp'=4,'tp'=4,'dp'=2] {'tp'}, dimensions={1}, use_global_device_ids=true | all-gather | bytes 30720 | tf_op jit(solution)/shard_map/all_gather | solution.py:96
  213.8 5.8 %multiply_convert_fusion = bf16[2,256,2048]{2,1,0:T(8,128)(2,1)} fusion(bf16[2,256,1024]{2,1,0:T(8,128)(2,1)S(1)} %bitcast.192, bf16[1024,2048]{1,0:T(8,128)(2,1)} %all-gather.2.cloned.1.call-done, f32[2,2048]{1,0:T(2,128)S(1)} %slice.72), kind=kOutput, calls=%fused_computation.58 | convolution fusion | flops 2149580800 | bytes 7356416 | tf_op jit(solution)/shard_map/snc,cd->snd/dot_general | solution.py:203
  (129 shorter events, 53.3 us)
Async XLA Ops:
  6.5 71.2 %copy-start = (bf16[2048,256]{1,0:T(8,128)(2,1)S(1)}, bf16[2048,256]{1,0:T(8,128)(2,1)}, u32[]{:S(2)}) copy-start(bf16[2048,256]{1,0:T(8,128)(2,1)} %param.24) | copy-start | bytes 3145732
  6.5 47.8 %copy-start.6 = (f32[2048]{0:T(1024)S(1)}, f32[2048]{0:T(1024)}, u32[]{:S(2)}) copy-start(f32[2048]{0:T(1024)} %param.20) | copy-start | bytes 24580
  6.5 47.8 %copy-start.5 = (bf16[2048,64]{0,1:T(8,128)(2,1)S(1)}, bf16[2048,64]{0,1:T(8,128)(2,1)}, u32[]{:S(2)}) copy-start(bf16[2048,64]{0,1:T(8,128)(2,1)} %param.25) | copy-start | bytes 786436
  6.5 207.2 %all-gather.2.cloned.1.call-start = ((), (), s32[]{:S(2)}) async-start(), calls=%async_computation.1 | async-start | bytes 5242880 | tf_op jit(solution)/shard_map/all_gather | solution.py:206
  54.4 6.1 %copy-start.4 = (bf16[2048,64]{0,1:T(8,128)(2,1)S(1)}, bf16[2048,64]{0,1:T(8,128)(2,1)}, u32[]{:S(2)}) copy-start(bf16[2048,64]{0,1:T(8,128)(2,1)} %param.26) | copy-start | bytes 786436
  67.5 33.2 %collective-permute-start = (bf16[2,128,128]{1,2,0:T(8,128)(2,1)S(1)}, bf16[2,128,128]{1,2,0:T(8,128)(2,1)S(1)}, u32[]{:S(2)}, u32[]{:S(2)}) collective-permute-start(bf16[2,128,128]{1,2,0:T(8,128)(2,1)S(1)} %get-tuple-element.191), channel_id=1, source_target_pairs={{0,8},{8,16},{16,24},{1,9},{9,17},{17,25},{2,10},{10,18},{18,26},{... | collective-permute-start | bytes 196616 | tf_op jit(solution)/shard_map/ppermute | solution.py:24
  68.8 31.9 %collective-permute-start.1 = (bf16[2,128,128]{1,2,0:T(8,128)(2,1)S(1)}, bf16[2,128,128]{1,2,0:T(8,128)(2,1)S(1)}, u32[]{:S(2)}, u32[]{:S(2)}) collective-permute-start(bf16[2,128,128]{1,2,0:T(8,128)(2,1)S(1)} %get-tuple-element.192), channel_id=1, source_target_pairs={{8,0},{16,8},{24,16},{9,1},{17,9},{25,17},{10,2},{18,10},{26,18},{... | collective-permute-start | bytes 196616 | tf_op jit(solution)/shard_map/ppermute | solution.py:26
  84.4 17.8 %copy-start.1 = (f32[4]{0:T(128)S(1)}, f32[4]{0:T(128)}, u32[]{:S(2)}) copy-start(f32[4]{0:T(128)} %param.29) | copy-start | bytes 52
  84.4 17.8 %copy-start.2 = (f32[4]{0:T(128)S(1)}, f32[4]{0:T(128)}, u32[]{:S(2)}) copy-start(f32[4]{0:T(128)} %param.28) | copy-start | bytes 52
  102.2 98.6 %copy-start.3 = (f32[3,512]{1,0:T(4,128)S(1)}, f32[3,512]{1,0:T(4,128)}, u32[]{:S(2)}) copy-start(f32[3,512]{1,0:T(4,128)} %get-tuple-element.180) | copy-start | bytes 18436
  113.4 6.7 %slice-start = ((s8[8388608]{0:T(1024)(128)(4,1)}), s8[4194304]{0:T(1024)(128)(4,1)S(1)}, s32[]{:S(2)}) async-start(s8[8388608]{0:T(1024)(128)(4,1)} %bitcast.186), calls=%async_computation.2 | async-start | bytes 8388608 | tf_op jit(solution)/shard_map/while
  113.4 6.7 %slice-start.1 = ((s8[8388608]{0:T(1024)(128)(4,1)}), s8[4194304]{0:T(1024)(128)(4,1)S(1)}, s32[]{:S(2)}) async-start(s8[8388608]{0:T(1024)(128)(4,1)} %bitcast.186), calls=%async_computation.3 | async-start | bytes 8388608 | tf_op jit(solution)/shard_map/while
  136.4 6.7 %slice-start = ((s8[8388608]{0:T(1024)(128)(4,1)}), s8[4194304]{0:T(1024)(128)(4,1)S(1)}, s32[]{:S(2)}) async-start(s8[8388608]{0:T(1024)(128)(4,1)} %bitcast.186), calls=%async_computation.2 | async-start | bytes 8388608 | tf_op jit(solution)/shard_map/while
  136.4 6.7 %slice-start.1 = ((s8[8388608]{0:T(1024)(128)(4,1)}), s8[4194304]{0:T(1024)(128)(4,1)S(1)}, s32[]{:S(2)}) async-start(s8[8388608]{0:T(1024)(128)(4,1)} %bitcast.186), calls=%async_computation.3 | async-start | bytes 8388608 | tf_op jit(solution)/shard_map/while
  159.3 6.7 %slice-start = ((s8[8388608]{0:T(1024)(128)(4,1)}), s8[4194304]{0:T(1024)(128)(4,1)S(1)}, s32[]{:S(2)}) async-start(s8[8388608]{0:T(1024)(128)(4,1)} %bitcast.186), calls=%async_computation.2 | async-start | bytes 8388608 | tf_op jit(solution)/shard_map/while
  159.3 6.7 %slice-start.1 = ((s8[8388608]{0:T(1024)(128)(4,1)}), s8[4194304]{0:T(1024)(128)(4,1)S(1)}, s32[]{:S(2)}) async-start(s8[8388608]{0:T(1024)(128)(4,1)} %bitcast.186), calls=%async_computation.3 | async-start | bytes 8388608 | tf_op jit(solution)/shard_map/while
  182.2 6.7 %slice-start = ((s8[8388608]{0:T(1024)(128)(4,1)}), s8[4194304]{0:T(1024)(128)(4,1)S(1)}, s32[]{:S(2)}) async-start(s8[8388608]{0:T(1024)(128)(4,1)} %bitcast.186), calls=%async_computation.2 | async-start | bytes 8388608 | tf_op jit(solution)/shard_map/while
  182.2 6.7 %slice-start.1 = ((s8[8388608]{0:T(1024)(128)(4,1)}), s8[4194304]{0:T(1024)(128)(4,1)S(1)}, s32[]{:S(2)}) async-start(s8[8388608]{0:T(1024)(128)(4,1)} %bitcast.186), calls=%async_computation.3 | async-start | bytes 8388608 | tf_op jit(solution)/shard_map/while
  197.3 16.2 %all-to-all-start = ((bf16[2,1024,256]{2,0,1:T(2,128)(2,1)}), bf16[2,1024,256]{2,0,1:T(2,128)(2,1)S(1)}, u32[]{:S(2)}, u32[]{:S(2)}) async-start(bf16[2,1024,256]{2,0,1:T(2,128)(2,1)} %copy.27), calls=%async_computation | async-start | bytes 2097152 | tf_op jit(solution)/shard_map/all_to_all | solution.py:202
Sparse Core Ops, SparseCore 0:
  70.4 52.5 all-gather.1
where the time goes:
time: 227 us; the launch traced here: 226 us
  matrix products  74.6 us (33%)
  blocking collectives  66.1 us (29%)
  other arithmetic  38.5 us (17%)
  local copies, waits for them, and re-layouts  17.8 us (8%)
  between operations  13.7 us (6%)
  loops' own time  9.49 us (4%)
  starting transfers between devices  6.28 us (3%)
    psum x1, blocking collectives, shards(): lax.psum((jnp.dot(active, w_shift, preferred_element_type=jnp.float32), j...  21.3 us
    reduce_sum x4, other arithmetic, attend(): far_exp.sum(-1, keepdims=True)  21 us
    dot_general x4, matrix products, attend(): jnp.einsum('qgrd,kgd->grqk', q_rows, far_keys, preferred_element_type=jnp...  18.3 us
    all_gather x1, blocking collectives, shards(): lax.all_gather(jnp.concatenate([ctx_keys, ctx_values], axis=-1), 'sp', ax...  15.8 us
    all_gather x1, blocking collectives, shards(): lax.all_gather(gate_part, 'tp', axis=1, tiled=True)  12.7 us
    another operation x1, loops' own time, shards(): lax.map(attend, jnp.arange(samples * blocks, dtype=jnp.int32))  9.49 us
    dot_general x4, matrix products, attend(): jnp.einsum('grqk,kgd->qgrd', (far_exp / normaliser).astype(jnp.bfloat16),...  8.49 us
    all_gather x1, blocking collectives, shards(): lax.all_gather(shift_part, 'tp', axis=1, tiled=True)  8.18 us
  transfers between devices with their start and end apart: 4, of which 0 were waited for; matrix products, arithmetic and copies ran while one was open for 45% of the time, Pallas kernels for 0%

commit v1 on v0

v1 whole, which is shorter than its diff:
```python
import functools

import jax
import jax.numpy as jnp
from jax import lax
from jax.experimental import pallas as pl
from jax.experimental.pallas import tpu as pltpu
from jax.sharding import PartitionSpec as P

HEAD = 64
WINDOW = 128
GRID_COLS = 64
LANES = 128

epsilon = 1e-06
rope_base = 10000.0
masked_value = -1e30
LOG2E = 1.4426950408889634
DIRECT = 4

f32 = jnp.float32
bf16 = jnp.bfloat16


def shifted(piece, axis, hop):
    count = lax.axis_size(axis)
    return lax.ppermute(piece, axis, [(i, (i + hop) % count) for i in range(count)])


def mod_kernel(cond_ref, shift_ref, scale_ref, gate_ref, out_ref):
    rows = cond_ref[...].astype(f32)
    active = (rows / (1.0 + jnp.exp(-rows))).astype(bf16)
    width = shift_ref.shape[1]
    for slot, weight in enumerate((shift_ref, scale_ref, gate_ref)):
        out_ref[:, slot * width : (slot + 1) * width] = jnp.dot(
            active, weight[...], preferred_element_type=f32
        )


def modulation(condition, ctx_cond, w_shift, w_scale, w_gate):
    rows = jnp.concatenate([condition, ctx_cond[None, :]], axis=0)
    part = pl.pallas_call(
        mod_kernel,
        out_shape=jax.ShapeDtypeStruct((rows.shape[0], 3 * w_shift.shape[1]), f32),
        name="mod_part",
    )(rows, w_shift, w_scale, w_gate)
    sp_count = lax.axis_size("sp")
    tp_count = lax.axis_size("tp")
    if sp_count <= DIRECT:
        pieces = [part] + [shifted(part, "sp", hop) for hop in range(1, sp_count)]
        part = functools.reduce(lambda a, b: a + b, pieces)
    else:
        part = lax.psum(part, "sp")
    part = part.reshape(rows.shape[0], 3, -1)
    width = part.shape[2]
    if tp_count <= DIRECT:
        mine = lax.axis_index("tp")
        full = jnp.zeros(part.shape[:2] + (width * tp_count,), f32)
        for hop in range(tp_count):
            piece = shifted(part, "tp", hop) if hop else part
            full = lax.dynamic_update_slice_in_dim(
                full, piece, ((mine - hop) % tp_count) * width, 2
            )
    else:
        full = lax.all_gather(part, "tp", axis=2, tiled=True)
    return full


def normed(rows, gain_row, shift_row):
    widened = rows.astype(f32)
    inverse = lax.rsqrt(jnp.mean(widened * widened, axis=-1, keepdims=True) + epsilon)
    return (widened * inverse * gain_row + shift_row).astype(bf16)


def ctx_kernel(x_ref, gain_ref, shift_ref, wk_ref, wv_ref, out_ref, w_scr):
    @pl.when(pl.program_id(0) == 0)
    def _():
        w_scr[:, :HEAD] = wk_ref[...]
        w_scr[:, HEAD:] = wv_ref[...]

    hidden = normed(x_ref[0], gain_ref[...], shift_ref[...])
    out_ref[0] = jnp.dot(hidden, w_scr[...], preferred_element_type=f32).astype(bf16)


def ctx_pairs(context, gain_row, shift_row, w_key, w_value):
    samples, rows, width = context.shape
    return pl.pallas_call(
        ctx_kernel,
        grid=(samples,),
        in_specs=[
            pl.BlockSpec((1, rows, width), lambda s: (s, 0, 0)),
            pl.BlockSpec((1, width), lambda s: (0, 0)),
            pl.BlockSpec((1, width), lambda s: (0, 0)),
            pl.BlockSpec(w_key.shape, lambda s: (0, 0)),
            pl.BlockSpec(w_value.shape, lambda s: (0, 0)),
        ],
        out_specs=pl.BlockSpec((1, rows, 2 * HEAD), lambda s: (s, 0, 0)),
        out_shape=jax.ShapeDtypeStruct((samples, rows, 2 * HEAD), bf16),
        scratch_shapes=[pltpu.VMEM((width, 2 * HEAD), bf16)],
        name="ctx_proj",
    )(context, gain_row, shift_row, w_key, w_value)


def proj_kernel(
    x_ref, gain_ref, shift_ref, wq_ref, wk_ref, wv_ref, cos_ref, lo_ref, hi_ref,
    q_ref, kv_ref, w_scr,
):
    cols = wq_ref.shape[1]

    @pl.when(pl.program_id(0) == 0)
    def _():
        w_scr[:, :cols] = wq_ref[...]
        w_scr[:, cols : cols + HEAD] = wk_ref[...]
        w_scr[:, cols + HEAD :] = wv_ref[...]

    hidden = normed(x_ref[0], gain_ref[...], shift_ref[...])
    product = jnp.dot(hidden, w_scr[...], preferred_element_type=f32)
    cosine, low, high = cos_ref[...], lo_ref[...], hi_ref[...]

    def rotated(part):
        return (
            part * cosine
            + pltpu.roll(part, LANES - HEAD // 4, 1) * low
            + pltpu.roll(part, HEAD // 4, 1) * high
        )

    for start in range(0, cols, LANES):
        part = product[:, start : start + LANES]
        q_ref[:, start : start + LANES] = (rotated(part) * (LOG2E * HEAD**-0.5)).astype(bf16)
    part = product[:, cols:]
    lane = lax.broadcasted_iota(jnp.int32, part.shape, 1)
    kv_ref[...] = jnp.where(lane < HEAD, rotated(part), part).astype(bf16)


def projected_rows(latent, sample, gain_row, shift_row, w_query, w_key, w_value, tables):
    _, tokens, width = latent.shape
    block = min(256, tokens)
    cols = w_query.shape[1]
    table = pl.BlockSpec((block, LANES), lambda t: (t, 0))
    return pl.pallas_call(
        proj_kernel,
        grid=(tokens // block,),
        in_specs=[
            pl.BlockSpec((1, block, width), lambda t: (sample, t, 0)),
            pl.BlockSpec((1, width), lambda t: (0, 0)),
            pl.BlockSpec((1, width), lambda t: (0, 0)),
            pl.BlockSpec(w_query.shape, lambda t: (0, 0)),
            pl.BlockSpec(w_key.shape, lambda t: (0, 0)),
            pl.BlockSpec(w_value.shape, lambda t: (0, 0)),
            table,
            table,
            table,
        ],
        out_specs=[
            pl.BlockSpec((block, cols), lambda t: (t, 0)),
            pl.BlockSpec((block, 2 * HEAD), lambda t: (t, 0)),
        ],
        out_shape=[
            jax.ShapeDtypeStruct((tokens, cols), bf16),
            jax.ShapeDtypeStruct((tokens, 2 * HEAD), bf16),
        ],
        scratch_shapes=[pltpu.VMEM((width, cols + 2 * HEAD), bf16)],
        name="latent_proj",
    )(latent, gain_row, shift_row, w_query, w_key, w_value, *tables)


def rope_tables(tokens, offset):
    quarter = HEAD // 4
    positions = offset + jnp.arange(tokens, dtype=jnp.int32)
    frequency = rope_base ** (-jnp.arange(quarter, dtype=f32) / quarter)
    row_angle = (positions // GRID_COLS).astype(f32)[:, None] * frequency
    col_angle = (positions % GRID_COLS).astype(f32)[:, None] * frequency
    angles = jnp.concatenate([row_angle, col_angle], axis=1)
    cosine, sine = jnp.cos(angles), jnp.sin(angles)
    none = jnp.zeros((tokens, quarter), f32)
    c_row, c_col = cosine[:, :quarter], cosine[:, quarter:]
    s_row, s_col = sine[:, :quarter], sine[:, quarter:]
    twice = LANES // HEAD
    return (
        jnp.concatenate([c_row, c_row, c_col, c_col] * twice, axis=1),
        jnp.concatenate([-s_row, none, -s_col, none] * twice, axis=1),
        jnp.concatenate([none, s_row, none, s_col] * twice, axis=1),
    )


def attend_kernel(place_ref, lift_ref, sink_ref, q_ref, kv_ref, left_ref, right_ref, *rest, pieces, last_place):
    ctx_refs = rest[:pieces]
    out_ref, near_scr, nearv_scr, ctx_scr, ctxv_scr = rest[pieces:]
    step = pl.program_id(0)
    tokens = kv_ref.shape[0]
    piece_rows = ctx_refs[0].shape[1]
    block = q_ref.shape[0]
    heads = q_ref.shape[1] // HEAD

    @pl.when(step == 0)
    def _():
        near_scr[:WINDOW] = left_ref[...]
        near_scr[WINDOW : WINDOW + tokens] = kv_ref[...]
        near_scr[WINDOW + tokens :] = right_ref[...]
        for number, ref in enumerate(ctx_refs):
            ctx_scr[number * piece_rows : (number + 1) * piece_rows] = ref[0]
        for source, target in ((near_scr, nearv_scr), (ctx_scr, ctxv_scr)):
            turned = pltpu.roll(source[...].astype(f32), HEAD, 1)
            lane = lax.broadcasted_iota(jnp.int32, turned.shape, 1)
            target[...] = jnp.where(lane < HEAD, turned, 1.0).astype(bf16)

    ctx_rows, ctx_values = ctx_scr[...], ctxv_scr[...]
    row = lax.broadcasted_iota(jnp.int32, (WINDOW, WINDOW), 0)
    col = lax.broadcasted_iota(jnp.int32, (WINDOW, WINDOW), 1)
    contract = (((1,), (1,)), ((), ()))
    for sub in range(block // WINDOW):
        start = pl.multiple_of(step * block + sub * WINDOW, WINDOW)
        near_rows = near_scr[pl.ds(start, 3 * WINDOW), :]
        near_values = nearv_scr[pl.ds(start, 3 * WINDOW), :]
        left_from = jnp.where((place_ref[0] == 0) & (start == 0), 2 * WINDOW, 0)
        right_from = jnp.where(
            (place_ref[0] == last_place) & (start + WINDOW == tokens), 2 * WINDOW, 0
        )
        left_ok = col >= row + left_from
        right_ok = col + right_from <= row
        stacked = []
        lane = lax.broadcasted_iota(jnp.int32, (WINDOW, LANES), 1)
        for head in range(heads):
            chunk = q_ref[sub * WINDOW : (sub + 1) * WINDOW, head // 2 * LANES : head // 2 * LANES + LANES].astype(f32)
            if head % 2:
                chunk = pltpu.roll(chunk, HEAD, 1)
            stacked.append(jnp.where(lane < HEAD, chunk, 0.0).astype(bf16))
        stacked = jnp.concatenate(stacked, axis=0)
        far = lax.dot_general(stacked, ctx_rows, contract, preferred_element_type=f32)
        near = lax.dot_general(stacked, near_rows, contract, preferred_element_type=f32)
        outs = []
        for head in range(heads):
            span = slice(head * WINDOW, (head + 1) * WINDOW)
            lift = lift_ref[head] * LOG2E
            sink = sink_ref[head] * LOG2E
            far_h = far[span]
            near_h = near[span]
            near_l = jnp.where(left_ok, near_h[:, :WINDOW], masked_value)
            near_m = near_h[:, WINDOW : 2 * WINDOW]
            near_r = jnp.where(right_ok, near_h[:, 2 * WINDOW :], masked_value)
            near_max = jnp.maximum(jnp.maximum(near_l, near_m), near_r).max(-1, keepdims=True)
            top = jnp.maximum(
                jnp.maximum(near_max, far_h.max(-1, keepdims=True) + lift), sink
            )
            far_exp = jnp.exp2(far_h - (top - lift)).astype(bf16)
            near_exp = jnp.concatenate(
                [jnp.exp2(part - top).astype(bf16) for part in (near_l, near_m, near_r)], axis=1
            )
            acc = jnp.dot(far_exp, ctx_values, preferred_element_type=f32) + jnp.dot(
                near_exp, near_values, preferred_element_type=f32
            )
            total = pltpu.roll(acc, HEAD, 1) + jnp.exp2(sink - top)
            outs.append(acc / total)
        for pair in range(heads // 2):
            both = jnp.where(lane < HEAD, outs[2 * pair], pltpu.roll(outs[2 * pair + 1], HEAD, 1))
            out_ref[0, sub * WINDOW : (sub + 1) * WINDOW, pair * LANES : (pair + 1) * LANES] = both.astype(bf16)


def attended_rows(place, lift, sink, queries, pairs, left, right, ctx_pieces, sample, tp_count):
    tokens, cols = queries.shape
    block = tokens // tp_count
    pieces = len(ctx_pieces)
    piece_rows = ctx_pieces[0].shape[1]
    whole = lambda t, *_: (0, 0)
    grid_spec = pltpu.PrefetchScalarGridSpec(
        num_scalar_prefetch=3,
        grid=(tp_count,),
        in_specs=[
            pl.BlockSpec((block, cols), lambda t, *_: (t, 0)),
            pl.BlockSpec(pairs.shape, whole),
            pl.BlockSpec(left.shape, whole),
            pl.BlockSpec(right.shape, whole),
        ]
        + [pl.BlockSpec((1, piece_rows, 2 * HEAD), lambda t, *_: (sample, 0, 0))] * pieces,
        out_specs=pl.BlockSpec(
            (1, block, cols), lambda t, place, *_: (lax.rem(t - place[1] + tp_count, tp_count), 0, 0)
        ),
        scratch_shapes=[
            pltpu.VMEM((tokens + 2 * WINDOW, 2 * HEAD), bf16),
            pltpu.VMEM((tokens + 2 * WINDOW, 2 * HEAD), bf16),
            pltpu.VMEM((pieces * piece_rows, 2 * HEAD), bf16),
            pltpu.VMEM((pieces * piece_rows, 2 * HEAD), bf16),
        ],
    )
    return pl.pallas_call(
        functools.partial(attend_kernel, pieces=pieces, last_place=lax.axis_size("sp") - 1),
        grid_spec=grid_spec,
        out_shape=jax.ShapeDtypeStruct((tp_count, block, cols), bf16),
        name="attend",
    )(place, lift, sink, queries, pairs, left, right, *ctx_pieces)


def out_kernel(place_ref, *refs, hops):
    gate_ref = refs[0]
    pieces = refs[1 : 1 + hops]
    own_w = refs[1 + hops]
    near_w = refs[2 + hops : 1 + 2 * hops]
    far_w = refs[1 + 2 * hops : 3 * hops]
    out_ref = refs[-1]
    acc = jnp.dot(pieces[0][0], own_w[...], preferred_element_type=f32)
    first = place_ref[2] == 0
    for hop in range(1, hops):
        rows = pieces[hop][0]
        half = rows.shape[1] // 2
        low, high = rows[:, :half].astype(f32), rows[:, half:].astype(f32)
        mine = jnp.where(first, low, high).astype(bf16)
        other = jnp.where(first, high, low).astype(bf16)
        acc += jnp.dot(mine, near_w[hop - 1][...], preferred_element_type=f32)
        acc += jnp.dot(other, far_w[hop - 1][...], preferred_element_type=f32)
    out_ref[0] = (gate_ref[...] * acc).astype(bf16)


def out_rows(place, gate_row, pieces, own_w, near_w, far_w, sample, samples, previous):
    hops = len(pieces)
    block, cols = pieces[0].shape[1:]
    width = own_w.shape[1]
    tile = min(512, width)
    specs = [pl.BlockSpec((1, tile), lambda n, *_: (0, n))]
    specs += [pl.BlockSpec((1, block, cols), lambda n, *_: (0, 0, 0))] * hops
    specs += [pl.BlockSpec((cols, tile), lambda n, *_: (0, n))]
    specs += [pl.BlockSpec((cols // 2, tile), lambda n, *_: (0, n))] * (2 * (hops - 1))
    args = [gate_row, *pieces, own_w, *near_w, *far_w]
    aliases = {}
    if previous is not None:
        specs.append(pl.BlockSpec(memory_space=pl.ANY))
        args.append(previous)
        aliases = {len(args): 0}
    return pl.pallas_call(
        functools.partial(out_kernel, hops=hops),
        grid_spec=pltpu.PrefetchScalarGridSpec(
            num_scalar_prefetch=1,
            grid=(width // tile,),
            in_specs=specs,
            out_specs=pl.BlockSpec((1, block, tile), lambda n, *_: (sample, 0, n)),
        ),
        out_shape=jax.ShapeDtypeStruct((samples, block, width), bf16),
        input_output_aliases=aliases,
        name="out_proj",
    )(place, *args)


def shards(
    latent,
    context,
    condition,
    ctx_cond,
    norm_gain,
    w_shift,
    w_scale,
    w_gate,
    w_query,
    w_key,
    w_value,
    w_out,
    sink_logit,
    ctx_lift,
):
    samples, tokens, model_width = latent.shape
    sp_count = lax.axis_size("sp")
    tp_count = lax.axis_size("tp")
    place = jnp.stack(
        [lax.axis_index("sp"), lax.axis_index("tp"), lax.axis_index("dp")]
    ).astype(jnp.int32)
    tables = rope_tables(tokens, lax.axis_index("sp") * tokens)
    vectors = modulation(condition, ctx_cond, w_shift, w_scale, w_gate)
    gain = norm_gain * (1.0 + vectors[:, 1])
    shift, gate = vectors[:, 0], vectors[:, 2]

    ctx_own = ctx_pairs(context, gain[samples][None], shift[samples][None], w_key, w_value)
    if sp_count <= DIRECT:
        ctx_pieces = [ctx_own] + [shifted(ctx_own, "sp", hop) for hop in range(1, sp_count)]
    else:
        ctx_pieces = [lax.all_gather(ctx_own, "sp", axis=1, tiled=True)]

    half = w_out.shape[0] // 2
    w_out_late, _ = lax.optimization_barrier((w_out, gain))
    w_half = lax.dynamic_slice_in_dim(w_out_late, lax.axis_index("dp") * half, half, 0)
    near_w = [shifted(w_half, "tp", hop) for hop in range(1, tp_count)]
    far_w = [shifted(piece, "dp", 1) for piece in near_w]

    rows = []
    for sample in range(samples):
        queries, pairs = projected_rows(
            latent, sample, gain[sample][None], shift[sample][None], w_query, w_key, w_value, tables
        )
        left = lax.ppermute(pairs[-WINDOW:], "sp", [(i, i + 1) for i in range(sp_count - 1)])
        right = lax.ppermute(pairs[:WINDOW], "sp", [(i + 1, i) for i in range(sp_count - 1)])
        rows.append((queries, pairs, left, right))
    arrived = []
    for sample in range(samples):
        queries, pairs, left, right = rows[sample]
        attended = attended_rows(
            place, ctx_lift, sink_logit, queries, pairs, left, right, ctx_pieces, sample, tp_count
        )
        arrived.append(
            [attended[:1]] + [shifted(attended[hop : hop + 1], "tp", hop) for hop in range(1, tp_count)]
        )
    mixed = None
    for sample in range(samples):
        mixed = out_rows(
            place, gate[sample][None], arrived[sample], w_out, near_w, far_w, sample, samples, mixed
        )
    return mixed


def solution(mesh):
    return jax.shard_map(
        shards,
        mesh=mesh,
        in_specs=(
            P("dp", "sp", None),
            P("dp", "sp", None),
            P("dp", "sp"),
            P("sp"),
            P(),
            P("sp", "tp"),
            P("sp", "tp"),
            P("sp", "tp"),
            P(None, "tp"),
            P(None, "tp"),
            P(None, "tp"),
            P("tp", None),
            P("tp"),
            P("tp"),
        ),
        out_specs=P("dp", ("sp", "tp"), None),
        check_vma=False,
    )
```

time: 227 us -> 143 us (0.63)
  matrix products: 74.6 us -> 0 us
  blocking collectives: 66.1 us -> 0 us
  Pallas kernels: 0 us -> 59.2 us
  other arithmetic: 38.5 us -> 2.24 us
  starting transfers between devices: 6.28 us -> 37 us
  waiting for transfers between devices: 0.05 us -> 17 us
  between operations: 13.7 us -> 0.34 us
  loops' own time: 9.49 us -> 0 us
  local copies, waits for them, and re-layouts: 17.8 us -> 26.7 us
    dot_general x25 -> x0, matrix products: 74.6 us -> none  [the longest x4 18.3 us: attend(): jnp.einsum('qgrd,kgd->grqk', q_rows, far_keys, preferred_element_type=jnp...]
    pallas_call x0 -> x8, Pallas kernels: none -> 59.2 us  [the longest x2 24.3 us: attended_rows(): pl.pallas_call(functools.partial(attend_kernel, pieces=pieces, last_place...]
    all_gather x4 -> x0, blocking collectives: 44.8 us -> none  [the longest x1 15.8 us: shards(): lax.all_gather(jnp.concatenate([ctx_keys, ctx_values], axis=-1), 'sp', ax...]
    ppermute x2 -> x25, starting transfers between devices: 2.77 us -> 37 us  [the longest x21 30.2 us: shifted(): lax.ppermute(piece, axis, [(i, (i + hop) % count) for i in range(count)])]
    reduce_sum x10 -> x0, other arithmetic: 33.7 us -> none  [the longest x4 21 us: attend(): far_exp.sum(-1, keepdims=True)]
    psum x1 -> x0, blocking collectives: 21.3 us -> none  [shards(): lax.psum((jnp.dot(active, w_shift, preferred_element_type=jnp.float32), j...]
    ppermute x2 -> x25, waiting for transfers between devices: 0.01 us -> 17 us  [the longest x2 10.2 us: shards(): lax.ppermute(pairs[:WINDOW], 'sp', [(i + 1, i) for i in range(sp_count -...]
    concatenate x0 -> x4, local copies, waits for them, and re-layouts: none -> 11.2 us  [the longest x1 4.23 us: rope_tables(): jnp.concatenate([none, s_row, none, s_col] * twice, axis=1)]
  transfers between devices with their start and end apart: 4 -> 25, of which waited for: 0 -> 8; matrix products, arithmetic and copies ran while one was open for 45% -> 16% of each run, Pallas kernels for 0% -> 36%
where the time goes in v1:
time: 143 us; the launch traced here: 142 us
  Pallas kernels  59.2 us (41%)
  starting transfers between devices  37 us (26%)
  local copies, waits for them, and re-layouts  26.7 us (19%)
  waiting for transfers between devices  17 us (12%)
  other arithmetic  2.24 us (2%)
    ppermute x21, starting transfers between devices, shifted(): lax.ppermute(piece, axis, [(i, (i + hop) % count) for i in range(count)])  30.2 us
    pallas_call x2, Pallas kernels, attended_rows(): pl.pallas_call(functools.partial(attend_kernel, pieces=pieces, last_place...  24.3 us
    pallas_call x2, Pallas kernels, projected_rows(): pl.pallas_call(proj_kernel, grid=(tokens // block,), in_specs=[pl.BlockSp...  16 us
    pallas_call x2, Pallas kernels, out_rows(): pl.pallas_call(functools.partial(out_kernel, hops=hops), grid_spec=pltpu....  12.6 us
    ppermute x2, waiting for transfers between devices, shards(): lax.ppermute(pairs[:WINDOW], 'sp', [(i + 1, i) for i in range(sp_count -...  10.2 us
    unnamed x44, local copies, waits for them, and re-layouts  5.21 us
    concatenate x1, local copies, waits for them, and re-layouts, rope_tables(): jnp.concatenate([none, s_row, none, s_col] * twice, axis=1)  4.23 us
    concatenate x1, local copies, waits for them, and re-layouts, rope_tables(): jnp.concatenate([-s_row, none, -s_col, none] * twice, axis=1)  4.23 us
  transfers between devices with their start and end apart: 25, of which 8 were waited for; matrix products, arithmetic and copies ran while one was open for 16% of the time, Pallas kernels for 36%

profile of v1, /device:TPU:0, one launch (start us, length us, event | category | flops | bytes accessed | tf_op | source)
XLA Modules:
  0.0 142.4 jit_solution(10029695983538439242)
XLA Ops:
  2.0 2.3 %mod_part.1 = f32[3,1536]{1,0:T(4,128)} custom-call(bf16[3,512]{1,0:T(4,128)(2,1)} %pad_maximum_fusion.1.cond_ref, bf16[512,512]{1,0:T(8,128)(2,1)} %shift_ref.1, bf16[512,512]{1,0:T(8,128)(2,1)} %scale_ref.1, bf16[512,512]{1,0:T(8,128)(2,1)} %gate_ref.1), custom_call_target="tpu_custom_call" | custom-call | tf_op jit(solution)/shard_map/mod_part/pallas_call | solution.py:42
  4.3 5.1 %collective-permute-start.2 = (f32[3,1536]{1,0:T(4,128)}, f32[3,1536]{1,0:T(4,128)S(1)}, u32[]{:S(2)}, u32[]{:S(2)}) collective-permute-start(f32[3,1536]{1,0:T(4,128)} %mod_part.1), channel_id=1, source_target_pairs={{0,24},{8,0},{16,8},{24,16},{1,25},{9,1},{17,9},{25,17},{2,26},{10... | collective-permute-start | bytes 55304 | tf_op jit(solution)/shard_map/ppermute | solution.py:27
  10.7 1.9 %fusion.12 = (f32[1024,32]{1,0:T(8,128)S(1)}, f32[1024,32]{1,0:T(8,128)S(1)}) fusion(f32[1024,32]{1,0:T(8,128)S(1)} %copy.22), kind=kLoop, calls=%fused_computation.39 | loop fusion | bytes 393216 | tf_op jit(solution)/shard_map/sin | solution.py:174
  14.8 2.0 %copy.25.wv_ref = bf16[2048,64]{1,0:T(8,128)(2,1)} copy(bf16[2048,64]{0,1:T(8,128)(2,1)} %param.24) | data formatting | bytes 524288 | tf_op args[10]
  16.7 2.6 %concatenate.17.cos_ref = f32[1024,128]{1,0:T(8,128)} concatenate(f32[1024,16]{1,0:T(8,128)} %get-tuple-element.30, f32[1024,32]{1,0:T(8,128)S(1)} %get-tuple-element.28, f32[1024,16]{1,0:T(8,128)S(1)} %get-tuple-element.29, f32[1024,16]{1,0:T(8,128)} %get-tuple-element.30, f32[1024,32]{1,0:T(8,128)S(1)} %get-tuple-element.28, f32[1024,16]{1,0:T(8,128)S(1)} %get-tuple-element.29), dimensions={1} | concatenate | bytes 1048576 | tf_op jit(solution)/shard_map/concatenate | solution.py:180
  19.3 4.2 %concatenate.18.lo_ref = f32[1024,128]{1,0:T(8,128)} concatenate(f32[1024,16]{1,0:T(8,128)S(1)} %get-tuple-element.24, f32[1024,16]{1,0:T(8,128)S(1)} %broadcast_in_dim.16, f32[1024,16]{1,0:T(8,128)S(1)} %get-tuple-element.25, f32[1024,16]{1,0:T(8,128)S(1)} %broadcast_in_dim.16, f32[1024,16]{1,0:T(8,128)S(1)} %get-tuple-element.24, f32[1024,16]{1,0:T(8,128)S(1)} %broadcast_in_dim.16, ...), dimensions={1} | concatenate | bytes 1048576 | tf_op jit(solution)/shard_map/concatenate | solution.py:181
  23.6 4.2 %concatenate.19.hi_ref = f32[1024,128]{1,0:T(8,128)} concatenate(f32[1024,16]{1,0:T(8,128)S(1)} %broadcast_in_dim.16, f32[1024,16]{1,0:T(8,128)S(1)} %get-tuple-element.26, f32[1024,16]{1,0:T(8,128)S(1)} %broadcast_in_dim.16, f32[1024,16]{1,0:T(8,128)S(1)} %get-tuple-element.23, f32[1024,16]{1,0:T(8,128)S(1)} %broadcast_in_dim.16, f32[1024,16]{1,0:T(8,128)S(1)} %get-tuple-element.26, ...), dimensions={1} | concatenate | bytes 1048576 | tf_op jit(solution)/shard_map/concatenate | solution.py:182
  39.6 3.9 %ctx_proj.1.rest_0_ = bf16[2,256,128]{2,1,0:T(8,128)(2,1)} custom-call(bf16[2,256,2048]{2,1,0:T(8,128)(2,1)} %x_ref.4, f32[1,2048]{1,0:T(1,128)} %get-tuple-element.41.gain_ref, f32[1,2048]{1,0:T(1,128)} %get-tuple-element.37.shift_ref, bf16[2048,64]{1,0:T(8,128)(2,1)} %copy.24.wk_ref, bf16[2048,64]{1,0:T(8,128)(2,1)} %copy.25.wv_ref), custom_call_target="tpu_custom_call" | custom-call | tf_op jit(solution)/shard_map/ctx_proj/pallas_call | solution.py:87
  43.5 2.5 %collective-permute-start.8 = (bf16[2,256,128]{2,1,0:T(8,128)(2,1)}, bf16[2,256,128]{2,1,0:T(8,128)(2,1)S(1)}, u32[]{:S(2)}, u32[]{:S(2)}) collective-permute-start(bf16[2,256,128]{2,1,0:T(8,128)(2,1)} %ctx_proj.1.rest_0_), channel_id=1, source_target_pairs={{0,8},{8,16},{16,24},{24,0},{1,9},{9,17},{17,25},{25,1},{2,10},{10... | collective-permute-start | bytes 393224 | tf_op jit(solution)/shard_map/ppermute | solution.py:27
  46.0 8.0 %latent_proj.3 = (bf16[1024,256]{1,0:T(8,128)(2,1)}, bf16[1024,128]{1,0:T(8,128)(2,1)}) custom-call(bf16[2,1024,2048]{2,1,0:T(8,128)(2,1)} %x_ref.5, f32[1,2048]{1,0:T(1,128)} %get-tuple-element.40.gain_ref, f32[1,2048]{1,0:T(1,128)} %get-tuple-element.35.shift_ref, bf16[2048,256]{1,0:T(8,128)(2,1)} %wq_ref.3, bf16[2048,64]{1,0:T(8,128)(2,1)} %copy.24.wk_ref, ...), custom_call_target="tpu_custom_call" | custom-call | tf_op jit(solution)/shard_map/latent_proj/pallas_call | solution.py:140
  54.8 1.9 %collective-permute-start.20 = (bf16[128,128]{1,0:T(8,128)(2,1)S(1)}, bf16[128,128]{1,0:T(8,128)(2,1)S(1)}, u32[]{:S(2)}, u32[]{:S(2)}) collective-permute-start(bf16[128,128]{1,0:T(8,128)(2,1)S(1)} %get-tuple-element.32), channel_id=1, source_target_pairs={{0,8},{8,16},{16,24},{1,9},{9,17},{17,25},{2,10},{10,18},{18,26},{... | collective-permute-start | bytes 98312 | tf_op jit(solution)/shard_map/ppermute | solution.py:386
  59.6 5.4 %collective-permute-done.21.right_ref = bf16[128,128]{1,0:T(8,128)(2,1)S(1)} collective-permute-done((bf16[128,128]{1,0:T(8,128)(2,1)S(1)}, bf16[128,128]{1,0:T(8,128)(2,1)S(1)}, u32[]{:S(2)}, u32[]{:S(2)}) %collective-permute-start.21) | collective-permute-done | bytes 32800 | tf_op jit(solution)/shard_map/ppermute | solution.py:387
  64.9 2.7 %collective-permute-start.9 = (bf16[2,256,128]{2,1,0:T(8,128)(2,1)S(1)}, bf16[2,256,128]{2,1,0:T(8,128)(2,1)S(1)}, u32[]{:S(2)}, u32[]{:S(2)}) collective-permute-start(bf16[2,256,128]{2,1,0:T(8,128)(2,1)S(1)} %copy-done.7), channel_id=1, source_target_pairs={{0,16},{8,24},{16,0},{24,8},{1,17},{9,25},{17,1},{25,9},{2,18},{10... | collective-permute-start | bytes 393224 | tf_op jit(solution)/shard_map/ppermute | solution.py:27
  69.9 8.0 %latent_proj.2 = (bf16[1024,256]{1,0:T(8,128)(2,1)}, bf16[1024,128]{1,0:T(8,128)(2,1)}) custom-call(bf16[2,1024,2048]{2,1,0:T(8,128)(2,1)} %x_ref.5, f32[1,2048]{1,0:T(1,128)} %get-tuple-element.42.gain_ref, f32[1,2048]{1,0:T(1,128)} %get-tuple-element.38.shift_ref, bf16[2048,256]{1,0:T(8,128)(2,1)} %wq_ref.3, bf16[2048,64]{1,0:T(8,128)(2,1)} %copy.24.wk_ref, ...), custom_call_target="tpu_custom_call" | custom-call | tf_op jit(solution)/shard_map/latent_proj/pallas_call | solution.py:140
  78.6 12.2 %attend.3 = bf16[4,256,256]{2,1,0:T(8,128)(2,1)} custom-call(s32[3]{0:T(128)} %pad_add_fusion.place_ref, f32[4]{0:T(128)} %lift_ref.3, f32[4]{0:T(128)} %sink_ref.3, bf16[1024,256]{1,0:T(8,128)(2,1)} %get-tuple-element.13.q_ref, bf16[1024,128]{1,0:T(8,128)(2,1)} %get-tuple-element.14.kv_ref, bf16[128,128]{1,0:T(8,128)(2,1)} %copy-done.16, ...), custom_call_target="tpu_custom_call" | custom-call | tf_op jit(solution)/shard_map/attend/pallas_call | solution.py:285
  90.8 1.8 %fusion.9 = (bf16[1,256,256]{2,1,0:T(8,128)(2,1)}, bf16[1,256,256]{2,1,0:T(8,128)(2,1)}, bf16[1,256,256]{2,1,0:T(8,128)(2,1)S(1)}, bf16[1,256,256]{2,1,0:T(8,128)(2,1)}) fusion(bf16[4,256,256]{2,1,0:T(8,128)(2,1)} %attend.3), kind=kLoop, calls=%fused_computation.36 | loop fusion | bytes 1048576 | tf_op jit(solution)/shard_map/slice | solution.py:396
  95.6 2.3 %collective-permute-start.6 = (bf16[128,128]{1,0:T(8,128)(2,1)S(1)}, bf16[128,128]{1,0:T(8,128)(2,1)S(1)}, u32[]{:S(2)}, u32[]{:S(2)}) collective-permute-start(bf16[128,128]{1,0:T(8,128)(2,1)S(1)} %get-tuple-element.34), channel_id=1, source_target_pairs={{0,8},{8,16},{16,24},{1,9},{9,17},{17,25},{2,10},{10,18},{18,26},{... | collective-permute-start | bytes 98312 | tf_op jit(solution)/shard_map/ppermute | solution.py:386
  100.8 4.8 %collective-permute-done.7.right_ref = bf16[128,128]{1,0:T(8,128)(2,1)S(1)} collective-permute-done((bf16[128,128]{1,0:T(8,128)(2,1)S(1)}, bf16[128,128]{1,0:T(8,128)(2,1)S(1)}, u32[]{:S(2)}, u32[]{:S(2)}) %collective-permute-start.7) | collective-permute-done | bytes 32800 | tf_op jit(solution)/shard_map/ppermute | solution.py:387
  106.7 12.2 %attend.2 = bf16[4,256,256]{2,1,0:T(8,128)(2,1)} custom-call(s32[3]{0:T(128)} %pad_add_fusion.place_ref, f32[4]{0:T(128)} %lift_ref.3, f32[4]{0:T(128)} %sink_ref.3, bf16[1024,256]{1,0:T(8,128)(2,1)} %get-tuple-element.10.q_ref, bf16[1024,128]{1,0:T(8,128)(2,1)} %get-tuple-element.11.kv_ref, bf16[128,128]{1,0:T(8,128)(2,1)} %copy-done.18, ...), custom_call_target="tpu_custom_call" | custom-call | tf_op jit(solution)/shard_map/attend/pallas_call | solution.py:285
  118.9 2.5 %collective-permute-start.24 = (bf16[1,256,256]{2,1,0:T(8,128)(2,1)}, bf16[1,256,256]{2,1,0:T(8,128)(2,1)S(1)}, u32[]{:S(2)}, u32[]{:S(2)}) collective-permute-start(bf16[1,256,256]{2,1,0:T(8,128)(2,1)} %get-tuple-element.15), channel_id=1, source_target_pairs={{0,6},{2,0},{4,2},{6,4},{1,7},{3,1},{5,3},{7,5},{8,14},{10,8},{12,... | collective-permute-start | bytes 393224 | tf_op jit(solution)/shard_map/ppermute | solution.py:27
  121.4 1.9 %fusion.10 = (bf16[1,256,256]{2,1,0:T(8,128)(2,1)}, bf16[1,256,256]{2,1,0:T(8,128)(2,1)}, bf16[1,256,256]{2,1,0:T(8,128)(2,1)}, bf16[1,256,256]{2,1,0:T(8,128)(2,1)}) fusion(bf16[4,256,256]{2,1,0:T(8,128)(2,1)} %attend.2), kind=kLoop, calls=%fused_computation.37 | loop fusion | bytes 1048576 | tf_op jit(solution)/shard_map/slice | solution.py:396
  125.9 2.9 %collective-permute-start.13 = (bf16[1,256,256]{2,1,0:T(8,128)(2,1)}, bf16[1,256,256]{2,1,0:T(8,128)(2,1)}, u32[]{:S(2)}, u32[]{:S(2)}) collective-permute-start(bf16[1,256,256]{2,1,0:T(8,128)(2,1)} %get-tuple-element.19), channel_id=1, source_target_pairs={{0,6},{2,0},{4,2},{6,4},{1,7},{3,1},{5,3},{7,5},{8,14},{10,8},{12,... | collective-permute-start | bytes 393224 | tf_op jit(solution)/shard_map/ppermute | solution.py:27
  129.8 6.3 %out_proj.2.refs_12_ = bf16[2,256,2048]{2,1,0:T(8,128)(2,1)} custom-call(s32[3]{0:T(128)} %pad_add_fusion.place_ref, f32[1,2048]{1,0:T(1,128)} %get-tuple-element.36.refs_0_, bf16[1,256,256]{2,1,0:T(8,128)(2,1)} %get-tuple-element.18.refs_1_, bf16[1,256,256]{2,1,0:T(8,128)(2,1)} %copy-done.12, bf16[1,256,256]{2,1,0:T(8,128)(2,1)} %copy-done.13, ...), custom_call_target="tpu_custom_call" | custom-call | tf_op jit(solution)/shard_map/out_proj/pallas_call | solution.py:328
  136.1 6.3 %out_proj.3 = bf16[2,256,2048]{2,1,0:T(8,128)(2,1)} custom-call(s32[3]{0:T(128)} %pad_add_fusion.place_ref, f32[1,2048]{1,0:T(1,128)} %get-tuple-element.39.refs_0_, bf16[1,256,256]{2,1,0:T(8,128)(2,1)} %get-tuple-element.22.refs_1_, bf16[1,256,256]{2,1,0:T(8,128)(2,1)} %collective-permute-done.11.refs_2_, ...), custom_call_target="tpu_custom_call", output_to_operand_aliasing={{}: (13, {})} | custom-call | tf_op jit(solution)/shard_map/out_proj/pallas_call | solution.py:328
  (107 shorter events, 34.2 us)
Async XLA Ops:
  4.3 23.5 %collective-permute-start.2 = (f32[3,1536]{1,0:T(4,128)}, f32[3,1536]{1,0:T(4,128)S(1)}, u32[]{:S(2)}, u32[]{:S(2)}) collective-permute-start(f32[3,1536]{1,0:T(4,128)} %mod_part.1), channel_id=1, source_target_pairs={{0,24},{8,0},{16,8},{24,16},{1,25},{9,1},{17,9},{25,17},{2,26},{10... | collective-permute-start | bytes 55304 | tf_op jit(solution)/shard_map/ppermute | solution.py:27
  9.4 18.5 %collective-permute-start.1 = (f32[3,1536]{1,0:T(4,128)}, f32[3,1536]{1,0:T(4,128)S(1)}, u32[]{:S(2)}, u32[]{:S(2)}) collective-permute-start(f32[3,1536]{1,0:T(4,128)} %mod_part.1), channel_id=1, source_target_pairs={{0,16},{8,24},{16,0},{24,8},{1,17},{9,25},{17,1},{25,9},{2,18},{10... | collective-permute-start | bytes 55304 | tf_op jit(solution)/shard_map/ppermute | solution.py:27
  9.4 18.5 %collective-permute-start = (f32[3,1536]{1,0:T(4,128)}, f32[3,1536]{1,0:T(4,128)S(1)}, u32[]{:S(2)}, u32[]{:S(2)}) collective-permute-start(f32[3,1536]{1,0:T(4,128)} %mod_part.1), channel_id=1, source_target_pairs={{0,8},{8,16},{16,24},{24,0},{1,9},{9,17},{17,25},{25,1},{2,10},{10... | collective-permute-start | bytes 55304 | tf_op jit(solution)/shard_map/ppermute | solution.py:27
  27.8 4.8 %collective-permute-start.3 = (f32[3,3,512]{2,0,1:T(4,128)S(1)}, f32[3,3,512]{2,0,1:T(4,128)S(1)}, u32[]{:S(2)}, u32[]{:S(2)}) collective-permute-start(f32[3,3,512]{2,0,1:T(4,128)S(1)} %bitcast.18), channel_id=1, source_target_pairs={{0,2},{2,4},{4,6},{6,0},{1,3},{3,5},{5,7},{7,1},{8,10},{10,12},{12... | collective-permute-start | bytes 55304 | tf_op jit(solution)/shard_map/ppermute | solution.py:27
  29.4 3.8 %collective-permute-start.4 = (f32[3,3,512]{2,0,1:T(4,128)S(1)}, f32[3,3,512]{2,0,1:T(4,128)S(1)}, u32[]{:S(2)}, u32[]{:S(2)}) collective-permute-start(f32[3,3,512]{2,0,1:T(4,128)S(1)} %bitcast.19), channel_id=1, source_target_pairs={{0,4},{2,6},{4,0},{6,2},{1,5},{3,7},{5,1},{7,3},{8,12},{10,14},{12... | collective-permute-start | bytes 55304 | tf_op jit(solution)/shard_map/ppermute | solution.py:27
  30.9 3.8 %collective-permute-start.5 = (f32[3,3,512]{2,0,1:T(4,128)S(1)}, f32[3,3,512]{2,0,1:T(4,128)S(1)}, u32[]{:S(2)}, u32[]{:S(2)}) collective-permute-start(f32[3,3,512]{2,0,1:T(4,128)S(1)} %bitcast.20), channel_id=1, source_target_pairs={{0,6},{2,0},{4,2},{6,4},{1,7},{3,1},{5,3},{7,5},{8,14},{10,8},{12,... | collective-permute-start | bytes 55304 | tf_op jit(solution)/shard_map/ppermute | solution.py:27
  36.1 58.1 %collective-permute-start.14 = (bf16[128,2048]{1,0:T(8,128)(2,1)S(1)}, bf16[128,2048]{1,0:T(8,128)(2,1)S(1)}, u32[]{:S(2)}, u32[]{:S(2)}) collective-permute-start(bf16[128,2048]{1,0:T(8,128)(2,1)S(1)} %constant_dynamic-slice_fusion), channel_id=1, source_target_pairs={{0,2},{2,4},{4,6},{6,0},{1,3},{3,5},{5,7},{7,1},{8,10},{10,12},{12... | collective-permute-start | bytes 1572872 | tf_op jit(solution)/shard_map/ppermute | solution.py:27
  37.5 56.6 %collective-permute-start.15 = (bf16[128,2048]{1,0:T(8,128)(2,1)S(1)}, bf16[128,2048]{1,0:T(8,128)(2,1)S(1)}, u32[]{:S(2)}, u32[]{:S(2)}) collective-permute-start(bf16[128,2048]{1,0:T(8,128)(2,1)S(1)} %constant_dynamic-slice_fusion), channel_id=1, source_target_pairs={{0,4},{2,6},{4,0},{6,2},{1,5},{3,7},{5,1},{7,3},{8,12},{10,14},{12... | collective-permute-start | bytes 1572872 | tf_op jit(solution)/shard_map/ppermute | solution.py:27
  39.0 55.6 %collective-permute-start.16 = (bf16[128,2048]{1,0:T(8,128)(2,1)S(1)}, bf16[128,2048]{1,0:T(8,128)(2,1)S(1)}, u32[]{:S(2)}, u32[]{:S(2)}) collective-permute-start(bf16[128,2048]{1,0:T(8,128)(2,1)S(1)} %constant_dynamic-slice_fusion), channel_id=1, source_target_pairs={{0,6},{2,0},{4,2},{6,4},{1,7},{3,1},{5,3},{7,5},{8,14},{10,8},{12,... | collective-permute-start | bytes 1572872 | tf_op jit(solution)/shard_map/ppermute | solution.py:27
  43.5 24.1 %collective-permute-start.8 = (bf16[2,256,128]{2,1,0:T(8,128)(2,1)}, bf16[2,256,128]{2,1,0:T(8,128)(2,1)S(1)}, u32[]{:S(2)}, u32[]{:S(2)}) collective-permute-start(bf16[2,256,128]{2,1,0:T(8,128)(2,1)} %ctx_proj.1.rest_0_), channel_id=1, source_target_pairs={{0,8},{8,16},{16,24},{24,0},{1,9},{9,17},{17,25},{25,1},{2,10},{10... | collective-permute-start | bytes 393224 | tf_op jit(solution)/shard_map/ppermute | solution.py:27
  58.3 6.7 %collective-permute-start.21 = (bf16[128,128]{1,0:T(8,128)(2,1)S(1)}, bf16[128,128]{1,0:T(8,128)(2,1)S(1)}, u32[]{:S(2)}, u32[]{:S(2)}) collective-permute-start(bf16[128,128]{1,0:T(8,128)(2,1)S(1)} %get-tuple-element.31), channel_id=1, source_target_pairs={{8,0},{16,8},{24,16},{9,1},{17,9},{25,17},{10,2},{18,10},{26,18},{... | collective-permute-start | bytes 98312 | tf_op jit(solution)/shard_map/ppermute | solution.py:387
  64.9 13.0 %collective-permute-start.9 = (bf16[2,256,128]{2,1,0:T(8,128)(2,1)S(1)}, bf16[2,256,128]{2,1,0:T(8,128)(2,1)S(1)}, u32[]{:S(2)}, u32[]{:S(2)}) collective-permute-start(bf16[2,256,128]{2,1,0:T(8,128)(2,1)S(1)} %copy-done.7), channel_id=1, source_target_pairs={{0,16},{8,24},{16,0},{24,8},{1,17},{9,25},{17,1},{25,9},{2,18},{10... | collective-permute-start | bytes 393224 | tf_op jit(solution)/shard_map/ppermute | solution.py:27
  67.6 10.3 %collective-permute-start.10 = (bf16[2,256,128]{2,1,0:T(8,128)(2,1)S(1)}, bf16[2,256,128]{2,1,0:T(8,128)(2,1)S(1)}, u32[]{:S(2)}, u32[]{:S(2)}) collective-permute-start(bf16[2,256,128]{2,1,0:T(8,128)(2,1)S(1)} %copy-done.7), channel_id=1, source_target_pairs={{0,24},{8,0},{16,8},{24,16},{1,25},{9,1},{17,9},{25,17},{2,26},{10... | collective-permute-start | bytes 393224 | tf_op jit(solution)/shard_map/ppermute | solution.py:27
  92.6 26.2 %collective-permute-start.22 = (bf16[1,256,256]{2,1,0:T(8,128)(2,1)S(1)}, bf16[1,256,256]{2,1,0:T(8,128)(2,1)S(1)}, u32[]{:S(2)}, u32[]{:S(2)}) collective-permute-start(bf16[1,256,256]{2,1,0:T(8,128)(2,1)S(1)} %get-tuple-element.17), channel_id=1, source_target_pairs={{0,2},{2,4},{4,6},{6,0},{1,3},{3,5},{5,7},{7,1},{8,10},{10,12},{12... | collective-permute-start | bytes 393224 | tf_op jit(solution)/shard_map/ppermute | solution.py:27
  94.1 31.8 %collective-permute-start.17 = (bf16[128,2048]{1,0:T(8,128)(2,1)S(1)}, bf16[128,2048]{1,0:T(8,128)(2,1)S(1)}, u32[]{:S(2)}, u32[]{:S(2)}) collective-permute-start(bf16[128,2048]{1,0:T(8,128)(2,1)S(1)} %collective-permute-done.14.refs_6_), channel_id=1, source_target_pairs={{0,1},{1,0},{2,3},{3,2},{4,5},{5,4},{6,7},{7,6},{8,9},{9,8},{10,11... | collective-permute-start | bytes 1572872 | tf_op jit(solution)/shard_map/ppermute | solution.py:27
  94.2 34.7 %collective-permute-start.18 = (bf16[128,2048]{1,0:T(8,128)(2,1)S(1)}, bf16[128,2048]{1,0:T(8,128)(2,1)S(1)}, u32[]{:S(2)}, u32[]{:S(2)}) collective-permute-start(bf16[128,2048]{1,0:T(8,128)(2,1)S(1)} %collective-permute-done.15.refs_7_), channel_id=1, source_target_pairs={{0,1},{1,0},{2,3},{3,2},{4,5},{5,4},{6,7},{7,6},{8,9},{9,8},{10,11... | collective-permute-start | bytes 1572872 | tf_op jit(solution)/shard_map/ppermute | solution.py:27
  94.6 34.2 %collective-permute-start.19 = (bf16[128,2048]{1,0:T(8,128)(2,1)S(1)}, bf16[128,2048]{1,0:T(8,128)(2,1)S(1)}, u32[]{:S(2)}, u32[]{:S(2)}) collective-permute-start(bf16[128,2048]{1,0:T(8,128)(2,1)S(1)} %collective-permute-done.16.refs_8_), channel_id=1, source_target_pairs={{0,1},{1,0},{2,3},{3,2},{4,5},{5,4},{6,7},{7,6},{8,9},{9,8},{10,11... | collective-permute-start | bytes 1572872 | tf_op jit(solution)/shard_map/ppermute | solution.py:27
  95.6 3.9 %collective-permute-start.6 = (bf16[128,128]{1,0:T(8,128)(2,1)S(1)}, bf16[128,128]{1,0:T(8,128)(2,1)S(1)}, u32[]{:S(2)}, u32[]{:S(2)}) collective-permute-start(bf16[128,128]{1,0:T(8,128)(2,1)S(1)} %get-tuple-element.34), channel_id=1, source_target_pairs={{0,8},{8,16},{16,24},{1,9},{9,17},{17,25},{2,10},{10,18},{18,26},{... | collective-permute-start | bytes 98312 | tf_op jit(solution)/shard_map/ppermute | solution.py:386
  99.5 6.1 %collective-permute-start.7 = (bf16[128,128]{1,0:T(8,128)(2,1)S(1)}, bf16[128,128]{1,0:T(8,128)(2,1)S(1)}, u32[]{:S(2)}, u32[]{:S(2)}) collective-permute-start(bf16[128,128]{1,0:T(8,128)(2,1)S(1)} %get-tuple-element.33), channel_id=1, source_target_pairs={{8,0},{16,8},{24,16},{9,1},{17,9},{25,17},{10,2},{18,10},{26,18},{... | collective-permute-start | bytes 98312 | tf_op jit(solution)/shard_map/ppermute | solution.py:387
  106.2 17.1 %collective-permute-start.23 = (bf16[1,256,256]{2,1,0:T(8,128)(2,1)}, bf16[1,256,256]{2,1,0:T(8,128)(2,1)S(1)}, u32[]{:S(2)}, u32[]{:S(2)}) collective-permute-start(bf16[1,256,256]{2,1,0:T(8,128)(2,1)} %get-tuple-element.16), channel_id=1, source_target_pairs={{0,4},{2,6},{4,0},{6,2},{1,5},{3,7},{5,1},{7,3},{8,12},{10,14},{12... | collective-permute-start | bytes 393224 | tf_op jit(solution)/shard_map/ppermute | solution.py:27
  118.9 5.8 %collective-permute-start.24 = (bf16[1,256,256]{2,1,0:T(8,128)(2,1)}, bf16[1,256,256]{2,1,0:T(8,128)(2,1)S(1)}, u32[]{:S(2)}, u32[]{:S(2)}) collective-permute-start(bf16[1,256,256]{2,1,0:T(8,128)(2,1)} %get-tuple-element.15), channel_id=1, source_target_pairs={{0,6},{2,0},{4,2},{6,4},{1,7},{3,1},{5,3},{7,5},{8,14},{10,8},{12,... | collective-permute-start | bytes 393224 | tf_op jit(solution)/shard_map/ppermute | solution.py:27
  123.3 12.8 %collective-permute-start.11 = (bf16[1,256,256]{2,1,0:T(8,128)(2,1)}, bf16[1,256,256]{2,1,0:T(8,128)(2,1)}, u32[]{:S(2)}, u32[]{:S(2)}) collective-permute-start(bf16[1,256,256]{2,1,0:T(8,128)(2,1)} %get-tuple-element.21), channel_id=1, source_target_pairs={{0,2},{2,4},{4,6},{6,0},{1,3},{3,5},{5,7},{7,1},{8,10},{10,12},{12... | collective-permute-start | bytes 393224 | tf_op jit(solution)/shard_map/ppermute | solution.py:27
  124.6 11.5 %collective-permute-start.12 = (bf16[1,256,256]{2,1,0:T(8,128)(2,1)}, bf16[1,256,256]{2,1,0:T(8,128)(2,1)}, u32[]{:S(2)}, u32[]{:S(2)}) collective-permute-start(bf16[1,256,256]{2,1,0:T(8,128)(2,1)} %get-tuple-element.20), channel_id=1, source_target_pairs={{0,4},{2,6},{4,0},{6,2},{1,5},{3,7},{5,1},{7,3},{8,12},{10,14},{12... | collective-permute-start | bytes 393224 | tf_op jit(solution)/shard_map/ppermute | solution.py:27
  125.9 10.2 %collective-permute-start.13 = (bf16[1,256,256]{2,1,0:T(8,128)(2,1)}, bf16[1,256,256]{2,1,0:T(8,128)(2,1)}, u32[]{:S(2)}, u32[]{:S(2)}) collective-permute-start(bf16[1,256,256]{2,1,0:T(8,128)(2,1)} %get-tuple-element.19), channel_id=1, source_target_pairs={{0,6},{2,0},{4,2},{6,4},{1,7},{3,1},{5,3},{7,5},{8,14},{10,8},{12,... | collective-permute-start | bytes 393224 | tf_op jit(solution)/shard_map/ppermute | solution.py:27
  (22 other events, 231.4 us)

commit v2 on v1

v2 whole, which is shorter than its diff:
```python
import functools

import jax
import jax.numpy as jnp
from jax import lax
from jax.experimental import pallas as pl
from jax.experimental.pallas import tpu as pltpu
from jax.sharding import PartitionSpec as P

HEAD = 64
WINDOW = 128
GRID_COLS = 64
LANES = 128

epsilon = 1e-06
rope_base = 10000.0
masked_value = -1e30
LOG2E = 1.4426950408889634
DIRECT = 4

f32 = jnp.float32
bf16 = jnp.bfloat16


def shifted(piece, axis, hop):
    count = lax.axis_size(axis)
    return lax.ppermute(piece, axis, [(i, (i + hop) % count) for i in range(count)])


def mod_kernel(cond_ref, ctx_ref, shift_ref, scale_ref, gate_ref, out_ref, rows_scr):
    samples = cond_ref.shape[0]
    rows_scr[:samples] = cond_ref[...].astype(f32)
    rows_scr[samples:] = ctx_ref[...].astype(f32)
    rows = rows_scr[...]
    active = (rows / (1.0 + jnp.exp(-rows))).astype(bf16)
    width = shift_ref.shape[1]
    for slot, weight in enumerate((shift_ref, scale_ref, gate_ref)):
        out_ref[:, slot * width : (slot + 1) * width] = jnp.dot(
            active, weight[...], preferred_element_type=f32
        )


def finish_kernel(place_ref, norm_ref, *refs, hops):
    gain_ref, shift_ref, gate_ref, sum_scr = refs[-4:]
    parts = refs[:-4]
    total = parts[0][...]
    for part in parts[1:]:
        total = total + part[...]
    rows = total.shape[1]
    width = total.shape[2] // 3
    for hop in range(hops):
        owner = lax.rem(place_ref[1] - hop + hops, hops)
        at = pl.ds(pl.multiple_of(owner * width, LANES), width)
        for slot in range(3):
            sum_scr[slot * rows : (slot + 1) * rows, at] = total[hop, :, slot * width : (slot + 1) * width]
    values = sum_scr[...]
    for row in range(rows):
        shift_ref[row] = values[row : row + 1]
        gain_ref[row] = norm_ref[...] * (1.0 + values[rows + row : rows + row + 1])
        gate_ref[row] = values[2 * rows + row : 2 * rows + row + 1]


def modulation(place, condition, ctx_cond, norm_gain, w_shift, w_scale, w_gate):
    rows = condition.shape[0] + 1
    width = w_shift.shape[1]
    part = pl.pallas_call(
        mod_kernel,
        out_shape=jax.ShapeDtypeStruct((rows, 3 * width), f32),
        scratch_shapes=[pltpu.VMEM((rows, condition.shape[1]), f32)],
        name="mod_part",
    )(condition, ctx_cond[None, :], w_shift, w_scale, w_gate)
    sp_count = lax.axis_size("sp")
    tp_count = lax.axis_size("tp")
    gathered = jnp.stack([part] + [shifted(part, "tp", hop) for hop in range(1, tp_count)])
    if sp_count <= DIRECT:
        parts = [gathered] + [shifted(gathered, "sp", hop) for hop in range(1, sp_count)]
    else:
        parts = [lax.psum(gathered, "sp")]
    model_width = norm_gain.shape[0]
    vector = jax.ShapeDtypeStruct((rows, 1, model_width), f32)
    smem = pl.BlockSpec(memory_space=pltpu.SMEM)
    vmem = pl.BlockSpec(memory_space=pltpu.VMEM)
    gain, shift, gate = pl.pallas_call(
        functools.partial(finish_kernel, hops=tp_count),
        in_specs=[smem, vmem] + [vmem] * len(parts),
        out_shape=[vector] * 3,
        scratch_shapes=[pltpu.VMEM((3 * rows, model_width), f32)],
        name="finish",
    )(place, norm_gain[None, :], *parts)
    return gain, shift, gate, gathered


def normed(rows, gain_row, shift_row):
    widened = rows.astype(f32)
    inverse = lax.rsqrt(jnp.mean(widened * widened, axis=-1, keepdims=True) + epsilon)
    return (widened * inverse * gain_row + shift_row).astype(bf16)


def small_tables(tokens, offset):
    quarter = HEAD // 4
    lane = jnp.arange(LANES, dtype=jnp.int32)[None, :]
    frequency = rope_base ** (-(lane % quarter).astype(f32) / quarter)
    groups = tokens // GRID_COLS
    number = jnp.arange(groups + GRID_COLS, dtype=jnp.int32)[:, None]
    of_row = number < groups
    turn = jnp.where(of_row, number + offset // GRID_COLS, number - groups).astype(f32)
    angle = turn * frequency
    used = of_row == (lane % HEAD < HEAD // 2)
    sign = jnp.where(lane // quarter % 2 == 0, -1.0, 1.0)
    return jnp.where(used, jnp.cos(angle), 0.0), jnp.where(used, jnp.sin(angle) * sign, 0.0)


def rotation(cos_ref, sin_ref, group, count):
    groups = cos_ref.shape[0] - GRID_COLS

    def table(ref):
        rows = [ref[pl.ds(group + i, 1), :] + ref[groups:, :] for i in range(count)]
        return jnp.concatenate(rows, axis=0)

    return table(cos_ref), table(sin_ref)


def rotated(part, cosine, sine):
    quarter = HEAD // 4
    lane = lax.broadcasted_iota(jnp.int32, part.shape, 1)
    partner = jnp.where(
        lane // quarter % 2 == 0,
        pltpu.roll(part, LANES - quarter, 1),
        pltpu.roll(part, quarter, 1),
    )
    return part * cosine + partner * sine


def rotated_pairs(part, cosine, sine):
    lane = lax.broadcasted_iota(jnp.int32, part.shape, 1)
    return jnp.where(lane < HEAD, rotated(part, cosine, sine), part).astype(bf16)


def early_kernel(
    x_ref, head_ref, tail_ref, gain_ref, shift_ref, cgain_ref, cshift_ref, wk_ref, wv_ref,
    cos_ref, sin_ref, ctx_ref, next_ref, prev_ref, w_scr,
):
    @pl.when(pl.program_id(0) == 0)
    def _():
        w_scr[:, :HEAD] = wk_ref[...]
        w_scr[:, HEAD:] = wv_ref[...]

    weights = w_scr[...]
    rows = x_ref.shape[1]
    groups = cos_ref.shape[0] - GRID_COLS
    edge = WINDOW // GRID_COLS
    hidden = normed(x_ref[0], cgain_ref[0], cshift_ref[0])
    ctx = jnp.dot(hidden, weights, preferred_element_type=f32).astype(bf16)
    ctx_ref[0] = ctx
    next_ref[0, :rows] = ctx
    prev_ref[0, :rows] = ctx
    for source, target, group in ((head_ref, prev_ref, 0), (tail_ref, next_ref, groups - edge)):
        hidden = normed(source[0], gain_ref[0], shift_ref[0])
        part = jnp.dot(hidden, weights, preferred_element_type=f32)
        target[0, rows:] = rotated_pairs(part, *rotation(cos_ref, sin_ref, group, edge))


def early_pairs(context, latent, gain, shift, w_key, w_value, tables):
    samples, rows, width = context.shape
    last = latent.shape[1] // WINDOW - 1
    vec = pl.BlockSpec((1, 1, width), lambda s: (s, 0, 0))
    ctx_vec = pl.BlockSpec((1, 1, width), lambda s: (samples, 0, 0))
    whole = lambda s: (0, 0)
    sizes = (rows, rows + WINDOW, rows + WINDOW)
    work = samples * (rows + 2 * WINDOW) * width
    return pl.pallas_call(
        early_kernel,
        grid=(samples,),
        in_specs=[
            pl.BlockSpec((1, rows, width), lambda s: (s, 0, 0)),
            pl.BlockSpec((1, WINDOW, width), lambda s: (s, 0, 0)),
            pl.BlockSpec((1, WINDOW, width), lambda s: (s, last, 0)),
            vec,
            vec,
            ctx_vec,
            ctx_vec,
            pl.BlockSpec(w_key.shape, whole),
            pl.BlockSpec(w_value.shape, whole),
            pl.BlockSpec(tables[0].shape, whole),
            pl.BlockSpec(tables[1].shape, whole),
        ],
        out_specs=[pl.BlockSpec((1, size, 2 * HEAD), lambda s: (s, 0, 0)) for size in sizes],
        out_shape=[jax.ShapeDtypeStruct((samples, size, 2 * HEAD), bf16) for size in sizes],
        scratch_shapes=[pltpu.VMEM((width, 2 * HEAD), bf16)],
        cost_estimate=pl.CostEstimate(flops=work * 4 * HEAD, transcendentals=0, bytes_accessed=2 * work),
        name="early_proj",
    )(context, latent, latent, gain, shift, gain, shift, w_key, w_value, *tables)


def proj_kernel(
    x_ref, gain_ref, shift_ref, wq_ref, wk_ref, wv_ref, cos_ref, sin_ref, q_ref, kv_ref, w_scr
):
    cols = wq_ref.shape[1]

    @pl.when((pl.program_id(0) == 0) & (pl.program_id(1) == 0))
    def _():
        w_scr[:, :cols] = wq_ref[...]
        w_scr[:, cols : cols + HEAD] = wk_ref[...]
        w_scr[:, cols + HEAD :] = wv_ref[...]

    count = x_ref.shape[1] // GRID_COLS
    hidden = normed(x_ref[0], gain_ref[0], shift_ref[0])
    product = jnp.dot(hidden, w_scr[...], preferred_element_type=f32)
    cosine, sine = rotation(cos_ref, sin_ref, pl.program_id(1) * count, count)
    for start in range(0, cols, LANES):
        part = rotated(product[:, start : start + LANES], cosine, sine)
        q_ref[0, :, start : start + LANES] = (part * (LOG2E * HEAD**-0.5)).astype(bf16)
    kv_ref[0] = rotated_pairs(product[:, cols:], cosine, sine)


def projected_rows(latent, gain, shift, w_query, w_key, w_value, tables):
    samples, tokens, width = latent.shape
    block = min(256, tokens)
    cols = w_query.shape[1]
    vec = pl.BlockSpec((1, 1, width), lambda s, t: (s, 0, 0))
    whole = lambda s, t: (0, 0)
    work = samples * tokens * width
    return pl.pallas_call(
        proj_kernel,
        grid=(samples, tokens // block),
        in_specs=[
            pl.BlockSpec((1, block, width), lambda s, t: (s, t, 0)),
            vec,
            vec,
            pl.BlockSpec(w_query.shape, whole),
            pl.BlockSpec(w_key.shape, whole),
            pl.BlockSpec(w_value.shape, whole),
            pl.BlockSpec(tables[0].shape, whole),
            pl.BlockSpec(tables[1].shape, whole),
        ],
        out_specs=[
            pl.BlockSpec((1, block, cols), lambda s, t: (s, t, 0)),
            pl.BlockSpec((1, block, 2 * HEAD), lambda s, t: (s, t, 0)),
        ],
        out_shape=[
            jax.ShapeDtypeStruct((samples, tokens, cols), bf16),
            jax.ShapeDtypeStruct((samples, tokens, 2 * HEAD), bf16),
        ],
        scratch_shapes=[pltpu.VMEM((width, cols + 2 * HEAD), bf16)],
        cost_estimate=pl.CostEstimate(
            flops=work * 2 * (cols + 2 * HEAD), transcendentals=0, bytes_accessed=2 * work
        ),
        name="latent_proj",
    )(latent, gain, shift, w_query, w_key, w_value, *tables)


def attend_kernel(place_ref, lift_ref, sink_ref, q_ref, kv_ref, left_ref, right_ref, *rest, pieces, last_place):
    ctx_refs = rest[:pieces]
    out_ref, near_scr, nearv_scr, ctx_scr, ctxv_scr = rest[pieces:]
    step = pl.program_id(0)
    tokens = kv_ref.shape[1]
    piece_rows = ctx_scr.shape[0] // pieces
    block = q_ref.shape[1]
    heads = q_ref.shape[2] // HEAD

    @pl.when(step == 0)
    def _():
        near_scr[:WINDOW] = left_ref[0, left_ref.shape[1] - WINDOW :]
        near_scr[WINDOW : WINDOW + tokens] = kv_ref[0]
        near_scr[WINDOW + tokens :] = right_ref[0, right_ref.shape[1] - WINDOW :]
        for number, ref in enumerate(ctx_refs):
            ctx_scr[number * piece_rows : (number + 1) * piece_rows] = ref[0, :piece_rows]
        for source, target in ((near_scr, nearv_scr), (ctx_scr, ctxv_scr)):
            turned = pltpu.roll(source[...].astype(f32), HEAD, 1)
            lane = lax.broadcasted_iota(jnp.int32, turned.shape, 1)
            target[...] = jnp.where(lane < HEAD, turned, 1.0).astype(bf16)

    ctx_rows, ctx_values = ctx_scr[...], ctxv_scr[...]
    row = lax.broadcasted_iota(jnp.int32, (WINDOW, WINDOW), 0)
    col = lax.broadcasted_iota(jnp.int32, (WINDOW, WINDOW), 1)
    contract = (((1,), (1,)), ((), ()))
    for sub in range(block // WINDOW):
        start = pl.multiple_of(step * block + sub * WINDOW, WINDOW)
        near_rows = near_scr[pl.ds(start, 3 * WINDOW), :]
        near_values = nearv_scr[pl.ds(start, 3 * WINDOW), :]
        left_from = jnp.where((place_ref[0] == 0) & (start == 0), 2 * WINDOW, 0)
        right_from = jnp.where(
            (place_ref[0] == last_place) & (start + WINDOW == tokens), 2 * WINDOW, 0
        )
        left_ok = col >= row + left_from
        right_ok = col + right_from <= row
        stacked = []
        lane = lax.broadcasted_iota(jnp.int32, (WINDOW, LANES), 1)
        for head in range(heads):
            chunk = q_ref[0, sub * WINDOW : (sub + 1) * WINDOW, head // 2 * LANES : head // 2 * LANES + LANES].astype(f32)
            if head % 2:
                chunk = pltpu.roll(chunk, HEAD, 1)
            stacked.append(jnp.where(lane < HEAD, chunk, 0.0).astype(bf16))
        stacked = jnp.concatenate(stacked, axis=0)
        far = lax.dot_general(stacked, ctx_rows, contract, preferred_element_type=f32)
        near = lax.dot_general(stacked, near_rows, contract, preferred_element_type=f32)
        outs = []
        for head in range(heads):
            span = slice(head * WINDOW, (head + 1) * WINDOW)
            lift = lift_ref[head] * LOG2E
            sink = sink_ref[head] * LOG2E
            far_h = far[span]
            near_h = near[span]
            near_l = jnp.where(left_ok, near_h[:, :WINDOW], masked_value)
            near_m = near_h[:, WINDOW : 2 * WINDOW]
            near_r = jnp.where(right_ok, near_h[:, 2 * WINDOW :], masked_value)
            near_max = jnp.maximum(jnp.maximum(near_l, near_m), near_r).max(-1, keepdims=True)
            top = jnp.maximum(
                jnp.maximum(near_max, far_h.max(-1, keepdims=True) + lift), sink
            )
            far_exp = jnp.exp2(far_h - (top - lift)).astype(bf16)
            near_exp = jnp.concatenate(
                [jnp.exp2(part - top).astype(bf16) for part in (near_l, near_m, near_r)], axis=1
            )
            acc = jnp.dot(far_exp, ctx_values, preferred_element_type=f32) + jnp.dot(
                near_exp, near_values, preferred_element_type=f32
            )
            total = pltpu.roll(acc, HEAD, 1) + jnp.exp2(sink - top)
            outs.append(acc / total)
        for pair in range(heads // 2):
            both = jnp.where(lane < HEAD, outs[2 * pair], pltpu.roll(outs[2 * pair + 1], HEAD, 1))
            out_ref[0, sub * WINDOW : (sub + 1) * WINDOW, pair * LANES : (pair + 1) * LANES] = both.astype(bf16)


def attended_rows(place, lift, sink, queries, pairs, left, right, ctx_pieces, sample, tp_count):
    _, tokens, cols = queries.shape
    block = tokens // tp_count
    pieces = len(ctx_pieces)
    piece_rows = ctx_pieces[0].shape[1]
    at_sample = lambda t, *_: (sample, 0, 0)
    whole_of = lambda array: pl.BlockSpec((1,) + array.shape[1:], at_sample)
    keys = pieces * piece_rows
    work = tokens * (keys + 3 * WINDOW) * cols
    grid_spec = pltpu.PrefetchScalarGridSpec(
        num_scalar_prefetch=3,
        grid=(tp_count,),
        in_specs=[pl.BlockSpec((1, block, cols), lambda t, *_: (sample, t, 0))]
        + [whole_of(array) for array in (pairs, left, right, *ctx_pieces)],
        out_specs=pl.BlockSpec(
            (1, block, cols), lambda t, place, *_: (lax.rem(t - place[1] + tp_count, tp_count), 0, 0)
        ),
        scratch_shapes=[
            pltpu.VMEM((tokens + 2 * WINDOW, 2 * HEAD), bf16),
            pltpu.VMEM((tokens + 2 * WINDOW, 2 * HEAD), bf16),
            pltpu.VMEM((keys, 2 * HEAD), bf16),
            pltpu.VMEM((keys, 2 * HEAD), bf16),
        ],
    )
    return pl.pallas_call(
        functools.partial(attend_kernel, pieces=pieces, last_place=lax.axis_size("sp") - 1),
        grid_spec=grid_spec,
        out_shape=jax.ShapeDtypeStruct((tp_count, block, cols), bf16),
        cost_estimate=pl.CostEstimate(flops=4 * work, transcendentals=0, bytes_accessed=work // keys),
        name="attend",
    )(place, lift, sink, queries, pairs, left, right, *ctx_pieces)


def out_kernel(place_ref, *refs, hops):
    gate_ref = refs[0]
    pieces = refs[1 : 1 + hops]
    own_w = refs[1 + hops]
    near_w = refs[2 + hops : 1 + 2 * hops]
    far_w = refs[1 + 2 * hops : 3 * hops]
    out_ref, lhs_scr = refs[-2:]
    first = place_ref[2] == 0

    @pl.when(pl.program_id(0) == 0)
    def _():
        cols = own_w.shape[0]
        lhs_scr[:, :cols] = pieces[0][0]
        for hop in range(1, hops):
            rows = pieces[hop][0]
            half = cols // 2
            low, high = rows[:, :half].astype(f32), rows[:, half:].astype(f32)
            at = hop * cols
            lhs_scr[:, at : at + half] = jnp.where(first, low, high).astype(bf16)
            lhs_scr[:, at + half : at + cols] = jnp.where(first, high, low).astype(bf16)

    blocks = [own_w[...]]
    for hop in range(1, hops):
        blocks += [near_w[hop - 1][...], far_w[hop - 1][...]]
    acc = jnp.dot(lhs_scr[...], jnp.concatenate(blocks, axis=0), preferred_element_type=f32)
    out_ref[0] = (gate_ref[0] * acc).astype(bf16)


def out_rows(place, gate, pieces, own_w, near_w, far_w, sample, samples, previous):
    hops = len(pieces)
    block, cols = pieces[0].shape[1:]
    width = own_w.shape[1]
    tile = min(512, width)
    specs = [pl.BlockSpec((1, 1, tile), lambda n, *_: (sample, 0, n))]
    specs += [pl.BlockSpec((1, block, cols), lambda n, *_: (0, 0, 0))] * hops
    specs += [pl.BlockSpec((cols, tile), lambda n, *_: (0, n))]
    specs += [pl.BlockSpec((cols // 2, tile), lambda n, *_: (0, n))] * (2 * (hops - 1))
    args = [gate, *pieces, own_w, *near_w, *far_w]
    aliases = {}
    if previous is not None:
        specs.append(pl.BlockSpec(memory_space=pl.ANY))
        args.append(previous)
        aliases = {len(args): 0}
    return pl.pallas_call(
        functools.partial(out_kernel, hops=hops),
        grid_spec=pltpu.PrefetchScalarGridSpec(
            num_scalar_prefetch=1,
            grid=(width // tile,),
            in_specs=specs,
            out_specs=pl.BlockSpec((1, block, tile), lambda n, *_: (sample, 0, n)),
            scratch_shapes=[pltpu.VMEM((block, hops * cols), bf16)],
        ),
        out_shape=jax.ShapeDtypeStruct((samples, block, width), bf16),
        input_output_aliases=aliases,
        cost_estimate=pl.CostEstimate(
            flops=2 * block * hops * cols * width, transcendentals=0, bytes_accessed=2 * hops * cols * width
        ),
        name="out_proj",
    )(place, *args)


def shards(
    latent,
    context,
    condition,
    ctx_cond,
    norm_gain,
    w_shift,
    w_scale,
    w_gate,
    w_query,
    w_key,
    w_value,
    w_out,
    sink_logit,
    ctx_lift,
):
    samples, tokens, model_width = latent.shape
    sp_count = lax.axis_size("sp")
    tp_count = lax.axis_size("tp")
    place = jnp.stack(
        [lax.axis_index("sp"), lax.axis_index("tp"), lax.axis_index("dp")]
    ).astype(jnp.int32)
    gain, shift, gate, first_stage = modulation(
        place, condition, ctx_cond, norm_gain, w_shift, w_scale, w_gate
    )
    w_late, offset = lax.optimization_barrier((w_out, place, first_stage))[:2]
    tables = small_tables(tokens, offset[0] * tokens)
    half = w_out.shape[0] // 2
    w_half = lax.dynamic_slice_in_dim(w_late, lax.axis_index("dp") * half, half, 0)
    near_w = [shifted(w_half, "tp", hop) for hop in range(1, tp_count)]
    far_w = [shifted(piece, "dp", 1) for piece in near_w]

    ctx_own, to_next, to_prev = early_pairs(context, latent, gain, shift, w_key, w_value, tables)
    rows = ctx_own.shape[1]
    if 3 <= sp_count <= DIRECT:
        left, right = shifted(to_next, "sp", 1), shifted(to_prev, "sp", sp_count - 1)
        ctx_pieces = [ctx_own, left, right]
        ctx_pieces += [shifted(ctx_own, "sp", hop) for hop in range(2, sp_count - 1)]
    else:
        left = shifted(to_next[:, rows:], "sp", 1)
        right = shifted(to_prev[:, rows:], "sp", sp_count - 1)
        ctx_pieces = [lax.all_gather(ctx_own, "sp", axis=1, tiled=True)]

    queries, pairs = projected_rows(latent, gain, shift, w_query, w_key, w_value, tables)
    arrived = []
    for sample in range(samples):
        attended = attended_rows(
            place, ctx_lift, sink_logit, queries, pairs, left, right, ctx_pieces, sample, tp_count
        )
        arrived.append(
            [attended[:1]] + [shifted(attended[hop : hop + 1], "tp", hop) for hop in range(1, tp_count)]
        )
    mixed = None
    for sample in range(samples):
        mixed = out_rows(place, gate, arrived[sample], w_out, near_w, far_w, sample, samples, mixed)
    return mixed


def solution(mesh):
    return jax.shard_map(
        shards,
        mesh=mesh,
        in_specs=(
            P("dp", "sp", None),
            P("dp", "sp", None),
            P("dp", "sp"),
            P("sp"),
            P(),
            P("sp", "tp"),
            P("sp", "tp"),
            P("sp", "tp"),
            P(None, "tp"),
            P(None, "tp"),
            P(None, "tp"),
            P("tp", None),
            P("tp"),
            P("tp"),
        ),
        out_specs=P("dp", ("sp", "tp"), None),
        check_vma=False,
    )
```

time: 143 us -> 110 us (0.77)
  local copies, waits for them, and re-layouts: 26.7 us -> 12.7 us
  starting transfers between devices: 37 us -> 26.1 us
  waiting for transfers between devices: 17 us -> 9.42 us
    ppermute x4 -> x0, waiting for transfers between devices: 13.3 us -> none  [the longest x2 10.2 us: shards(): lax.ppermute(pairs[:WINDOW], 'sp', [(i + 1, i) for i in range(sp_count -...]
    concatenate x4 -> x0, local copies, waits for them, and re-layouts: 11.2 us -> none  [the longest x1 4.23 us: rope_tables(): jnp.concatenate([none, s_row, none, s_col] * twice, axis=1)]
    ppermute x4 -> x0, starting transfers between devices: 6.76 us -> none  [the longest x2 4.2 us: shards(): lax.ppermute(pairs[-WINDOW:], 'sp', [(i, i + 1) for i in range(sp_count -...]
    ppermute x21, waiting for transfers between devices: 3.64 us -> 9.42 us  [shifted(): lax.ppermute(piece, axis, [(i, (i + hop) % count) for i in range(count)])]
    ppermute x21, starting transfers between devices: 30.2 us -> 26.1 us  [shifted(): lax.ppermute(piece, axis, [(i, (i + hop) % count) for i in range(count)])]
    slice x5 -> x0, local copies, waits for them, and re-layouts: 3.84 us -> none  [the longest x2 1.65 us: shards(): pairs[:WINDOW]]
    unnamed x44 -> x46, local copies, waits for them, and re-layouts: 5.21 us -> 7.51 us
    sin x1 -> x0, local copies, waits for them, and re-layouts: 1.86 us -> none  [rope_tables(): cosine, sine = (jnp.cos(angles), jnp.sin(angles))]
  transfers between devices with their start and end apart: 25 -> 21, of which waited for: 8 -> 5; matrix products, arithmetic and copies ran while one was open for 16% -> 7% of each run, Pallas kernels for 36% -> 39%
where the time goes in v2:
time: 110 us; the launch traced here: 109 us
  Pallas kernels  59 us (54%)
  starting transfers between devices  26.1 us (24%)
  local copies, waits for them, and re-layouts  12.7 us (12%)
  waiting for transfers between devices  9.42 us (9%)
  other arithmetic  1.71 us (2%)
    ppermute x21, starting transfers between devices, shifted(): lax.ppermute(piece, axis, [(i, (i + hop) % count) for i in range(count)])  26.1 us
    pallas_call x2, Pallas kernels, attended_rows(): pl.pallas_call(functools.partial(attend_kernel, pieces=pieces, last_place...  24.5 us
    pallas_call x1, Pallas kernels, projected_rows(): pl.pallas_call(proj_kernel, grid=(samples, tokens // block), in_specs=[pl...  12.7 us
    pallas_call x2, Pallas kernels, out_rows(): pl.pallas_call(functools.partial(out_kernel, hops=hops), grid_spec=pltpu....  11.9 us
    ppermute x21, waiting for transfers between devices, shifted(): lax.ppermute(piece, axis, [(i, (i + hop) % count) for i in range(count)])  9.42 us
    unnamed x46, local copies, waits for them, and re-layouts  7.51 us
    pallas_call x1, Pallas kernels, early_pairs(): pl.pallas_call(early_kernel, grid=(samples,), in_specs=[pl.BlockSpec((1,...  5.91 us
    slice x2, local copies, waits for them, and re-layouts, shards(): attended[hop:hop + 1]  3.85 us
  transfers between devices with their start and end apart: 21, of which 5 were waited for; matrix products, arithmetic and copies ran while one was open for 7% of the time, Pallas kernels for 39%

profile of v2, /device:TPU:0, one launch (start us, length us, event | category | flops | bytes accessed | tf_op | source)
XLA Modules:
  0.0 109.2 jit_solution(8108234535391598836)
XLA Ops:
  0.0 1.3 %broadcast_in_dim.22.ctx_ref = bf16[1,512]{1,0:T(2,128)(2,1)} reshape(bf16[512]{0:T(512)(128)(2,1)} %param.17) | data formatting | bytes 2048 | tf_op jit(solution)/shard_map/broadcast_in_dim | solution.py:71
  1.3 2.3 %mod_part.1 = f32[3,1536]{1,0:T(4,128)} custom-call(bf16[2,512]{1,0:T(2,128)(2,1)} %cond_ref.1, bf16[1,512]{1,0:T(2,128)(2,1)} %broadcast_in_dim.22.ctx_ref, bf16[512,512]{1,0:T(8,128)(2,1)} %shift_ref.1, bf16[512,512]{1,0:T(8,128)(2,1)} %scale_ref.1, bf16[512,512]{1,0:T(8,128)(2,1)} %gate_ref.1), custom_call_target="tpu_custom_call" | custom-call | tf_op jit(solution)/shard_map/mod_part/pallas_call | solution.py:66
  3.6 3.9 %collective-permute-start.2 = (f32[3,1536]{1,0:T(4,128)}, f32[3,1536]{1,0:T(4,128)S(1)}, u32[]{:S(2)}, u32[]{:S(2)}) collective-permute-start(f32[3,1536]{1,0:T(4,128)} %mod_part.1), channel_id=1, source_target_pairs={{0,6},{2,0},{4,2},{6,4},{1,7},{3,1},{5,3},{7,5},{8,14},{10,8},{12,... | collective-permute-start | bytes 55304 | tf_op jit(solution)/shard_map/ppermute | solution.py:27
  8.7 2.0 %copy.16.wk_ref = bf16[2048,64]{1,0:T(8,128)(2,1)} copy(bf16[2048,64]{0,1:T(8,128)(2,1)} %param.23) | data formatting | bytes 524288 | tf_op args[9]
  11.7 1.2 %collective-permute-done = f32[3,1536]{1,0:T(4,128)S(1)} collective-permute-done((f32[3,1536]{1,0:T(4,128)}, f32[3,1536]{1,0:T(4,128)S(1)}, u32[]{:S(2)}, u32[]{:S(2)}) %collective-permute-start) | collective-permute-done | bytes 18464 | tf_op jit(solution)/shard_map/ppermute | solution.py:27
  13.8 3.7 %collective-permute-start.5 = (f32[4,3,1536]{2,1,0:T(4,128)S(1)}, f32[4,3,1536]{2,1,0:T(4,128)S(1)}, u32[]{:S(2)}, u32[]{:S(2)}) collective-permute-start(f32[4,3,1536]{2,1,0:T(4,128)S(1)} %pad_maximum_fusion.refs_0_), channel_id=1, source_target_pairs={{0,24},{8,0},{16,8},{24,16},{1,25},{9,1},{17,9},{25,17},{2,26},{10... | collective-permute-start | bytes 221192 | tf_op jit(solution)/shard_map/ppermute | solution.py:27
  19.9 5.1 %collective-permute-done.4.refs_2_ = f32[4,3,1536]{2,1,0:T(4,128)S(1)} collective-permute-done((f32[4,3,1536]{2,1,0:T(4,128)S(1)}, f32[4,3,1536]{2,1,0:T(4,128)S(1)}, u32[]{:S(2)}, u32[]{:S(2)}) %collective-permute-start.4) | collective-permute-done | bytes 73760 | tf_op jit(solution)/shard_map/ppermute | solution.py:27
  25.7 1.7 %finish.1 = (f32[3,1,2048]{2,1,0:T(1,128)}, f32[3,1,2048]{2,1,0:T(1,128)}, f32[3,1,2048]{2,1,0:T(1,128)}) custom-call(s32[3]{0:T(128)} %copy-done.18, f32[1,2048]{1,0:T(1,128)} %bitcast.14, f32[4,3,1536]{2,1,0:T(4,128)} %copy-done.7, f32[4,3,1536]{2,1,0:T(4,128)} %copy-done.17, f32[4,3,1536]{2,1,0:T(4,128)} %copy-done.16, f32[4,3,1536]{2,1,0:T(4,128)} %copy-done.15), custom_call_target="tpu_custom_call" | custom-call | tf_op jit(solution)/shard_map/finish/pallas_call | solution.py:83
  27.4 5.9 %early_proj.1 = (bf16[2,256,128]{2,1,0:T(8,128)(2,1)}, bf16[2,384,128]{2,1,0:T(8,128)(2,1)}, bf16[2,384,128]{2,1,0:T(8,128)(2,1)}) custom-call(bf16[2,256,2048]{2,1,0:T(8,128)(2,1)} %x_ref.3, bf16[2,1024,2048]{2,1,0:T(8,128)(2,1)} %tail_ref.1, bf16[2,1024,2048]{2,1,0:T(8,128)(2,1)} %tail_ref.1, f32[3,1,2048]{2,1,0:T(1,128)} %get-tuple-element.16.gain_ref.cgain_ref, ...), custom_call_target="tpu_custom_call" | custom-call | flops 536870912 | bytes 4194304 | tf_op jit(solution)/shard_map/early_proj/pallas_call | solution.py:171
  33.3 1.7 %collective-permute-start.8 = (bf16[2,256,128]{2,1,0:T(8,128)(2,1)}, bf16[2,256,128]{2,1,0:T(8,128)(2,1)S(1)}, u32[]{:S(2)}, u32[]{:S(2)}) collective-permute-start(bf16[2,256,128]{2,1,0:T(8,128)(2,1)} %get-tuple-element.23.rest_0_), channel_id=1, source_target_pairs={{0,16},{8,24},{16,0},{24,8},{1,17},{9,25},{17,1},{25,9},{2,18},{10... | collective-permute-start | bytes 393224 | tf_op jit(solution)/shard_map/ppermute | solution.py:27
  35.1 2.0 %collective-permute-start.14 = (bf16[128,2048]{1,0:T(8,128)(2,1)S(1)}, bf16[128,2048]{1,0:T(8,128)(2,1)S(1)}, u32[]{:S(2)}, u32[]{:S(2)}) collective-permute-start(bf16[128,2048]{1,0:T(8,128)(2,1)S(1)} %constant_dynamic-slice_fusion), channel_id=1, source_target_pairs={{0,6},{2,0},{4,2},{6,4},{1,7},{3,1},{5,3},{7,5},{8,14},{10,8},{12,... | collective-permute-start | bytes 1572872 | tf_op jit(solution)/shard_map/ppermute | solution.py:27
  37.2 1.5 %collective-permute-start.13 = (bf16[128,2048]{1,0:T(8,128)(2,1)S(1)}, bf16[128,2048]{1,0:T(8,128)(2,1)S(1)}, u32[]{:S(2)}, u32[]{:S(2)}) collective-permute-start(bf16[128,2048]{1,0:T(8,128)(2,1)S(1)} %constant_dynamic-slice_fusion), channel_id=1, source_target_pairs={{0,4},{2,6},{4,0},{6,2},{1,5},{3,7},{5,1},{7,3},{8,12},{10,14},{12... | collective-permute-start | bytes 1572872 | tf_op jit(solution)/shard_map/ppermute | solution.py:27
  39.1 1.9 %collective-permute-done.8.rest_3_ = bf16[2,256,128]{2,1,0:T(8,128)(2,1)S(1)} collective-permute-done((bf16[2,256,128]{2,1,0:T(8,128)(2,1)}, bf16[2,256,128]{2,1,0:T(8,128)(2,1)S(1)}, u32[]{:S(2)}, u32[]{:S(2)}) %collective-permute-start.8) | collective-permute-done | bytes 131104 | tf_op jit(solution)/shard_map/ppermute | solution.py:27
  41.0 2.9 %collective-permute-start.7 = (bf16[2,384,128]{2,1,0:T(8,128)(2,1)}, bf16[2,384,128]{2,1,0:T(8,128)(2,1)S(1)}, u32[]{:S(2)}, u32[]{:S(2)}) collective-permute-start(bf16[2,384,128]{2,1,0:T(8,128)(2,1)} %get-tuple-element.22), channel_id=1, source_target_pairs={{0,24},{8,0},{16,8},{24,16},{1,25},{9,1},{17,9},{25,17},{2,26},{10... | collective-permute-start | bytes 589832 | tf_op jit(solution)/shard_map/ppermute | solution.py:27
  43.9 12.7 %latent_proj.1 = (bf16[2,1024,256]{2,1,0:T(8,128)(2,1)}, bf16[2,1024,128]{2,1,0:T(8,128)(2,1)}) custom-call(bf16[2,1024,2048]{2,1,0:T(8,128)(2,1)} %tail_ref.1, f32[3,1,2048]{2,1,0:T(1,128)} %get-tuple-element.16.gain_ref.cgain_ref, f32[3,1,2048]{2,1,0:T(1,128)} %get-tuple-element.17.shift_ref.cshift_ref, bf16[2048,256]{1,0:T(8,128)(2,1)} %wq_ref.1, ...), custom_call_target="tpu_custom_call" | custom-call | flops 3221225472 | bytes 8388608 | tf_op jit(solution)/shard_map/latent_proj/pallas_call | solution.py:223
  57.3 12.2 %attend.3 = bf16[4,256,256]{2,1,0:T(8,128)(2,1)} custom-call(s32[3]{0:T(128)} %copy-done.18, f32[4]{0:T(128)} %lift_ref.3, f32[4]{0:T(128)} %sink_ref.3, bf16[2,1024,256]{2,1,0:T(8,128)(2,1)} %get-tuple-element.19.q_ref, bf16[2,1024,128]{2,1,0:T(8,128)(2,1)} %get-tuple-element.20.kv_ref, bf16[2,384,128]{2,1,0:T(8,128)(2,1)} %copy-done.19, ...), custom_call_target="tpu_custom_call" | custom-call | flops 1476395008 | bytes 360448 | tf_op jit(solution)/shard_map/attend/pallas_call | solution.py:349
  70.3 1.9 %fusion.7 = (bf16[1,256,256]{2,1,0:T(8,128)(2,1)}, bf16[1,256,256]{2,1,0:T(8,128)(2,1)}, bf16[1,256,256]{2,1,0:T(8,128)(2,1)S(1)}, bf16[1,256,256]{2,1,0:T(8,128)(2,1)}) fusion(bf16[4,256,256]{2,1,0:T(8,128)(2,1)} %attend.3), kind=kLoop, calls=%fused_computation.26 | loop fusion | bytes 1048576 | tf_op jit(solution)/shard_map/slice | solution.py:469
  72.2 1.8 %collective-permute-start.20 = (bf16[1,256,256]{2,1,0:T(8,128)(2,1)}, bf16[1,256,256]{2,1,0:T(8,128)(2,1)S(1)}, u32[]{:S(2)}, u32[]{:S(2)}) collective-permute-start(bf16[1,256,256]{2,1,0:T(8,128)(2,1)} %get-tuple-element.25), channel_id=1, source_target_pairs={{0,6},{2,0},{4,2},{6,4},{1,7},{3,1},{5,3},{7,5},{8,14},{10,8},{12,... | collective-permute-start | bytes 393224 | tf_op jit(solution)/shard_map/ppermute | solution.py:27
  74.0 2.1 %collective-permute-start.19 = (bf16[1,256,256]{2,1,0:T(8,128)(2,1)}, bf16[1,256,256]{2,1,0:T(8,128)(2,1)S(1)}, u32[]{:S(2)}, u32[]{:S(2)}) collective-permute-start(bf16[1,256,256]{2,1,0:T(8,128)(2,1)} %get-tuple-element.26), channel_id=1, source_target_pairs={{0,4},{2,6},{4,0},{6,2},{1,5},{3,7},{5,1},{7,3},{8,12},{10,14},{12... | collective-permute-start | bytes 393224 | tf_op jit(solution)/shard_map/ppermute | solution.py:27
  76.1 12.2 %attend.2 = bf16[4,256,256]{2,1,0:T(8,128)(2,1)} custom-call(s32[3]{0:T(128)} %copy-done.18, f32[4]{0:T(128)} %lift_ref.3, f32[4]{0:T(128)} %sink_ref.3, bf16[2,1024,256]{2,1,0:T(8,128)(2,1)} %get-tuple-element.19.q_ref, bf16[2,1024,128]{2,1,0:T(8,128)(2,1)} %get-tuple-element.20.kv_ref, bf16[2,384,128]{2,1,0:T(8,128)(2,1)} %copy-done.19, ...), custom_call_target="tpu_custom_call" | custom-call | flops 1476395008 | bytes 360448 | tf_op jit(solution)/shard_map/attend/pallas_call | solution.py:349
  88.5 1.9 %fusion.8 = (bf16[1,256,256]{2,1,0:T(8,128)(2,1)}, bf16[1,256,256]{2,1,0:T(8,128)(2,1)}, bf16[1,256,256]{2,1,0:T(8,128)(2,1)}, bf16[1,256,256]{2,1,0:T(8,128)(2,1)}) fusion(bf16[4,256,256]{2,1,0:T(8,128)(2,1)} %attend.2), kind=kLoop, calls=%fused_computation.27 | loop fusion | bytes 1048576 | tf_op jit(solution)/shard_map/slice | solution.py:469
  91.0 2.9 %collective-permute-start.11 = (bf16[1,256,256]{2,1,0:T(8,128)(2,1)}, bf16[1,256,256]{2,1,0:T(8,128)(2,1)S(1)}, u32[]{:S(2)}, u32[]{:S(2)}) collective-permute-start(bf16[1,256,256]{2,1,0:T(8,128)(2,1)} %get-tuple-element.29), channel_id=1, source_target_pairs={{0,6},{2,0},{4,2},{6,4},{1,7},{3,1},{5,3},{7,5},{8,14},{10,8},{12,... | collective-permute-start | bytes 393224 | tf_op jit(solution)/shard_map/ppermute | solution.py:27
  96.6 5.9 %out_proj.2.refs_12_ = bf16[2,256,2048]{2,1,0:T(8,128)(2,1)} custom-call(s32[3]{0:T(128)} %copy-done.18, f32[3,1,2048]{2,1,0:T(1,128)} %get-tuple-element.15.refs_0_, bf16[1,256,256]{2,1,0:T(8,128)(2,1)} %get-tuple-element.28.refs_1_, bf16[1,256,256]{2,1,0:T(8,128)(2,1)} %copy-done.14, bf16[1,256,256]{2,1,0:T(8,128)(2,1)} %copy-done.13, ...), custom_call_target="tpu_custom_call" | custom-call | flops 1073741824 | bytes 4194304 | tf_op jit(solution)/shard_map/out_proj/pallas_call | solution.py:401
  103.3 5.9 %out_proj.3 = bf16[2,256,2048]{2,1,0:T(8,128)(2,1)} custom-call(s32[3]{0:T(128)} %copy-done.18, f32[3,1,2048]{2,1,0:T(1,128)} %get-tuple-element.15.refs_0_, bf16[1,256,256]{2,1,0:T(8,128)(2,1)} %get-tuple-element.32.refs_1_, bf16[1,256,256]{2,1,0:T(8,128)(2,1)} %copy-done.11, bf16[1,256,256]{2,1,0:T(8,128)(2,1)} %copy-done.10, ...), custom_call_target="tpu_custom_call", output_to_operand_aliasing={{}: (13, {})} | custom-call | flops 1073741824 | bytes 4194304 | tf_op jit(solution)/shard_map/out_proj/pallas_call | solution.py:401
  (83 shorter events, 12.1 us)
Async XLA Ops:
  3.6 8.1 %collective-permute-start.2 = (f32[3,1536]{1,0:T(4,128)}, f32[3,1536]{1,0:T(4,128)S(1)}, u32[]{:S(2)}, u32[]{:S(2)}) collective-permute-start(f32[3,1536]{1,0:T(4,128)} %mod_part.1), channel_id=1, source_target_pairs={{0,6},{2,0},{4,2},{6,4},{1,7},{3,1},{5,3},{7,5},{8,14},{10,8},{12,... | collective-permute-start | bytes 55304 | tf_op jit(solution)/shard_map/ppermute | solution.py:27
  7.5 4.2 %collective-permute-start.1 = (f32[3,1536]{1,0:T(4,128)}, f32[3,1536]{1,0:T(4,128)S(1)}, u32[]{:S(2)}, u32[]{:S(2)}) collective-permute-start(f32[3,1536]{1,0:T(4,128)} %mod_part.1), channel_id=1, source_target_pairs={{0,4},{2,6},{4,0},{6,2},{1,5},{3,7},{5,1},{7,3},{8,12},{10,14},{12... | collective-permute-start | bytes 55304 | tf_op jit(solution)/shard_map/ppermute | solution.py:27
  8.0 4.9 %collective-permute-start = (f32[3,1536]{1,0:T(4,128)}, f32[3,1536]{1,0:T(4,128)S(1)}, u32[]{:S(2)}, u32[]{:S(2)}) collective-permute-start(f32[3,1536]{1,0:T(4,128)} %mod_part.1), channel_id=1, source_target_pairs={{0,2},{2,4},{4,6},{6,0},{1,3},{3,5},{5,7},{7,1},{8,10},{10,12},{12... | collective-permute-start | bytes 55304 | tf_op jit(solution)/shard_map/ppermute | solution.py:27
  13.8 6.1 %collective-permute-start.5 = (f32[4,3,1536]{2,1,0:T(4,128)S(1)}, f32[4,3,1536]{2,1,0:T(4,128)S(1)}, u32[]{:S(2)}, u32[]{:S(2)}) collective-permute-start(f32[4,3,1536]{2,1,0:T(4,128)S(1)} %pad_maximum_fusion.refs_0_), channel_id=1, source_target_pairs={{0,24},{8,0},{16,8},{24,16},{1,25},{9,1},{17,9},{25,17},{2,26},{10... | collective-permute-start | bytes 221192 | tf_op jit(solution)/shard_map/ppermute | solution.py:27
  17.4 7.6 %collective-permute-start.4 = (f32[4,3,1536]{2,1,0:T(4,128)S(1)}, f32[4,3,1536]{2,1,0:T(4,128)S(1)}, u32[]{:S(2)}, u32[]{:S(2)}) collective-permute-start(f32[4,3,1536]{2,1,0:T(4,128)S(1)} %pad_maximum_fusion.refs_0_), channel_id=1, source_target_pairs={{0,16},{8,24},{16,0},{24,8},{1,17},{9,25},{17,1},{25,9},{2,18},{10... | collective-permute-start | bytes 221192 | tf_op jit(solution)/shard_map/ppermute | solution.py:27
  17.4 7.6 %collective-permute-start.3 = (f32[4,3,1536]{2,1,0:T(4,128)S(1)}, f32[4,3,1536]{2,1,0:T(4,128)S(1)}, u32[]{:S(2)}, u32[]{:S(2)}) collective-permute-start(f32[4,3,1536]{2,1,0:T(4,128)S(1)} %pad_maximum_fusion.refs_0_), channel_id=1, source_target_pairs={{0,8},{8,16},{16,24},{24,0},{1,9},{9,17},{17,25},{25,1},{2,10},{10... | collective-permute-start | bytes 221192 | tf_op jit(solution)/shard_map/ppermute | solution.py:27
  33.3 7.7 %collective-permute-start.8 = (bf16[2,256,128]{2,1,0:T(8,128)(2,1)}, bf16[2,256,128]{2,1,0:T(8,128)(2,1)S(1)}, u32[]{:S(2)}, u32[]{:S(2)}) collective-permute-start(bf16[2,256,128]{2,1,0:T(8,128)(2,1)} %get-tuple-element.23.rest_0_), channel_id=1, source_target_pairs={{0,16},{8,24},{16,0},{24,8},{1,17},{9,25},{17,1},{25,9},{2,18},{10... | collective-permute-start | bytes 393224 | tf_op jit(solution)/shard_map/ppermute | solution.py:27
  35.1 34.4 %collective-permute-start.14 = (bf16[128,2048]{1,0:T(8,128)(2,1)S(1)}, bf16[128,2048]{1,0:T(8,128)(2,1)S(1)}, u32[]{:S(2)}, u32[]{:S(2)}) collective-permute-start(bf16[128,2048]{1,0:T(8,128)(2,1)S(1)} %constant_dynamic-slice_fusion), channel_id=1, source_target_pairs={{0,6},{2,0},{4,2},{6,4},{1,7},{3,1},{5,3},{7,5},{8,14},{10,8},{12,... | collective-permute-start | bytes 1572872 | tf_op jit(solution)/shard_map/ppermute | solution.py:27
  37.2 32.5 %collective-permute-start.13 = (bf16[128,2048]{1,0:T(8,128)(2,1)S(1)}, bf16[128,2048]{1,0:T(8,128)(2,1)S(1)}, u32[]{:S(2)}, u32[]{:S(2)}) collective-permute-start(bf16[128,2048]{1,0:T(8,128)(2,1)S(1)} %constant_dynamic-slice_fusion), channel_id=1, source_target_pairs={{0,4},{2,6},{4,0},{6,2},{1,5},{3,7},{5,1},{7,3},{8,12},{10,14},{12... | collective-permute-start | bytes 1572872 | tf_op jit(solution)/shard_map/ppermute | solution.py:27
  38.7 31.5 %collective-permute-start.12 = (bf16[128,2048]{1,0:T(8,128)(2,1)S(1)}, bf16[128,2048]{1,0:T(8,128)(2,1)S(1)}, u32[]{:S(2)}, u32[]{:S(2)}) collective-permute-start(bf16[128,2048]{1,0:T(8,128)(2,1)S(1)} %constant_dynamic-slice_fusion), channel_id=1, source_target_pairs={{0,2},{2,4},{4,6},{6,0},{1,3},{3,5},{5,7},{7,1},{8,10},{10,12},{12... | collective-permute-start | bytes 1572872 | tf_op jit(solution)/shard_map/ppermute | solution.py:27
  38.7 17.8 %collective-permute-start.6 = (bf16[2,384,128]{2,1,0:T(8,128)(2,1)}, bf16[2,384,128]{2,1,0:T(8,128)(2,1)S(1)}, u32[]{:S(2)}, u32[]{:S(2)}) collective-permute-start(bf16[2,384,128]{2,1,0:T(8,128)(2,1)} %get-tuple-element.21), channel_id=1, source_target_pairs={{0,8},{8,16},{16,24},{24,0},{1,9},{9,17},{17,25},{25,1},{2,10},{10... | collective-permute-start | bytes 589832 | tf_op jit(solution)/shard_map/ppermute | solution.py:27
  41.0 15.6 %collective-permute-start.7 = (bf16[2,384,128]{2,1,0:T(8,128)(2,1)}, bf16[2,384,128]{2,1,0:T(8,128)(2,1)S(1)}, u32[]{:S(2)}, u32[]{:S(2)}) collective-permute-start(bf16[2,384,128]{2,1,0:T(8,128)(2,1)} %get-tuple-element.22), channel_id=1, source_target_pairs={{0,24},{8,0},{16,8},{24,16},{1,25},{9,1},{17,9},{25,17},{2,26},{10... | collective-permute-start | bytes 589832 | tf_op jit(solution)/shard_map/ppermute | solution.py:27
  69.6 18.8 %copy-start.1 = (bf16[128,2048]{1,0:T(8,128)(2,1)}, bf16[128,2048]{1,0:T(8,128)(2,1)S(1)}, u32[]{:S(2)}) copy-start(bf16[128,2048]{1,0:T(8,128)(2,1)S(1)} %collective-permute-done.14.refs_8_) | copy-start | bytes 1572868
  69.6 25.9 %collective-permute-start.17 = (bf16[128,2048]{1,0:T(8,128)(2,1)S(1)}, bf16[128,2048]{1,0:T(8,128)(2,1)S(1)}, u32[]{:S(2)}, u32[]{:S(2)}) collective-permute-start(bf16[128,2048]{1,0:T(8,128)(2,1)S(1)} %collective-permute-done.14.refs_8_), channel_id=1, source_target_pairs={{0,1},{1,0},{2,3},{3,2},{4,5},{5,4},{6,7},{7,6},{8,9},{9,8},{10,11... | collective-permute-start | bytes 1572872 | tf_op jit(solution)/shard_map/ppermute | solution.py:27
  69.7 18.7 %copy-start.2 = (bf16[128,2048]{1,0:T(8,128)(2,1)}, bf16[128,2048]{1,0:T(8,128)(2,1)S(1)}, u32[]{:S(2)}) copy-start(bf16[128,2048]{1,0:T(8,128)(2,1)S(1)} %collective-permute-done.13.refs_7_) | copy-start | bytes 1572868
  69.7 25.8 %collective-permute-start.16 = (bf16[128,2048]{1,0:T(8,128)(2,1)S(1)}, bf16[128,2048]{1,0:T(8,128)(2,1)S(1)}, u32[]{:S(2)}, u32[]{:S(2)}) collective-permute-start(bf16[128,2048]{1,0:T(8,128)(2,1)S(1)} %collective-permute-done.13.refs_7_), channel_id=1, source_target_pairs={{0,1},{1,0},{2,3},{3,2},{4,5},{5,4},{6,7},{7,6},{8,9},{9,8},{10,11... | collective-permute-start | bytes 1572872 | tf_op jit(solution)/shard_map/ppermute | solution.py:27
  70.2 18.2 %copy-start.3 = (bf16[128,2048]{1,0:T(8,128)(2,1)}, bf16[128,2048]{1,0:T(8,128)(2,1)S(1)}, u32[]{:S(2)}) copy-start(bf16[128,2048]{1,0:T(8,128)(2,1)S(1)} %collective-permute-done.12.refs_6_) | copy-start | bytes 1572868
  70.2 25.3 %collective-permute-start.15 = (bf16[128,2048]{1,0:T(8,128)(2,1)S(1)}, bf16[128,2048]{1,0:T(8,128)(2,1)S(1)}, u32[]{:S(2)}, u32[]{:S(2)}) collective-permute-start(bf16[128,2048]{1,0:T(8,128)(2,1)S(1)} %collective-permute-done.12.refs_6_), channel_id=1, source_target_pairs={{0,1},{1,0},{2,3},{3,2},{4,5},{5,4},{6,7},{7,6},{8,9},{9,8},{10,11... | collective-permute-start | bytes 1572872 | tf_op jit(solution)/shard_map/ppermute | solution.py:27
  72.2 16.2 %collective-permute-start.20 = (bf16[1,256,256]{2,1,0:T(8,128)(2,1)}, bf16[1,256,256]{2,1,0:T(8,128)(2,1)S(1)}, u32[]{:S(2)}, u32[]{:S(2)}) collective-permute-start(bf16[1,256,256]{2,1,0:T(8,128)(2,1)} %get-tuple-element.25), channel_id=1, source_target_pairs={{0,6},{2,0},{4,2},{6,4},{1,7},{3,1},{5,3},{7,5},{8,14},{10,8},{12,... | collective-permute-start | bytes 393224 | tf_op jit(solution)/shard_map/ppermute | solution.py:27
  74.0 16.3 %collective-permute-start.19 = (bf16[1,256,256]{2,1,0:T(8,128)(2,1)}, bf16[1,256,256]{2,1,0:T(8,128)(2,1)S(1)}, u32[]{:S(2)}, u32[]{:S(2)}) collective-permute-start(bf16[1,256,256]{2,1,0:T(8,128)(2,1)} %get-tuple-element.26), channel_id=1, source_target_pairs={{0,4},{2,6},{4,0},{6,2},{1,5},{3,7},{5,1},{7,3},{8,12},{10,14},{12... | collective-permute-start | bytes 393224 | tf_op jit(solution)/shard_map/ppermute | solution.py:27
  88.4 6.1 %collective-permute-start.18 = (bf16[1,256,256]{2,1,0:T(8,128)(2,1)S(1)}, bf16[1,256,256]{2,1,0:T(8,128)(2,1)S(1)}, u32[]{:S(2)}, u32[]{:S(2)}) collective-permute-start(bf16[1,256,256]{2,1,0:T(8,128)(2,1)S(1)} %get-tuple-element.27), channel_id=1, source_target_pairs={{0,2},{2,4},{4,6},{6,0},{1,3},{3,5},{5,7},{7,1},{8,10},{10,12},{12... | collective-permute-start | bytes 393224 | tf_op jit(solution)/shard_map/ppermute | solution.py:27
  91.0 11.5 %collective-permute-start.11 = (bf16[1,256,256]{2,1,0:T(8,128)(2,1)}, bf16[1,256,256]{2,1,0:T(8,128)(2,1)S(1)}, u32[]{:S(2)}, u32[]{:S(2)}) collective-permute-start(bf16[1,256,256]{2,1,0:T(8,128)(2,1)} %get-tuple-element.29), channel_id=1, source_target_pairs={{0,6},{2,0},{4,2},{6,4},{1,7},{3,1},{5,3},{7,5},{8,14},{10,8},{12,... | collective-permute-start | bytes 393224 | tf_op jit(solution)/shard_map/ppermute | solution.py:27
  95.2 7.4 %collective-permute-start.10 = (bf16[1,256,256]{2,1,0:T(8,128)(2,1)}, bf16[1,256,256]{2,1,0:T(8,128)(2,1)S(1)}, u32[]{:S(2)}, u32[]{:S(2)}) collective-permute-start(bf16[1,256,256]{2,1,0:T(8,128)(2,1)} %get-tuple-element.30), channel_id=1, source_target_pairs={{0,4},{2,6},{4,0},{6,2},{1,5},{3,7},{5,1},{7,3},{8,12},{10,14},{12... | collective-permute-start | bytes 393224 | tf_op jit(solution)/shard_map/ppermute | solution.py:27
  95.4 7.1 %collective-permute-start.9 = (bf16[1,256,256]{2,1,0:T(8,128)(2,1)}, bf16[1,256,256]{2,1,0:T(8,128)(2,1)S(1)}, u32[]{:S(2)}, u32[]{:S(2)}) collective-permute-start(bf16[1,256,256]{2,1,0:T(8,128)(2,1)} %get-tuple-element.31), channel_id=1, source_target_pairs={{0,2},{2,4},{4,6},{6,0},{1,3},{3,5},{5,7},{7,1},{8,10},{10,12},{12... | collective-permute-start | bytes 393224 | tf_op jit(solution)/shard_map/ppermute | solution.py:27
  (19 other events, 82.6 us)

commit v3 on v2

--- a/solution.py
+++ b/solution.py
@@ -355,65 +355,61 @@
     )(place, lift, sink, queries, pairs, left, right, *ctx_pieces)
 
 
-def out_kernel(place_ref, *refs, hops):
-    gate_ref = refs[0]
-    pieces = refs[1 : 1 + hops]
-    own_w = refs[1 + hops]
-    near_w = refs[2 + hops : 1 + 2 * hops]
-    far_w = refs[1 + 2 * hops : 3 * hops]
+def out_kernel(place_ref, gate_ref, *refs, hops, samples):
+    pieces = refs[: samples * hops]
+    weights = refs[samples * hops : -2]
     out_ref, lhs_scr = refs[-2:]
     first = place_ref[2] == 0
+    block = pieces[0].shape[1]
 
     @pl.when(pl.program_id(0) == 0)
     def _():
-        cols = own_w.shape[0]
-        lhs_scr[:, :cols] = pieces[0][0]
-        for hop in range(1, hops):
-            rows = pieces[hop][0]
-            half = cols // 2
-            low, high = rows[:, :half].astype(f32), rows[:, half:].astype(f32)
-            at = hop * cols
-            lhs_scr[:, at : at + half] = jnp.where(first, low, high).astype(bf16)
-            lhs_scr[:, at + half : at + cols] = jnp.where(first, high, low).astype(bf16)
-
-    blocks = [own_w[...]]
-    for hop in range(1, hops):
-        blocks += [near_w[hop - 1][...], far_w[hop - 1][...]]
-    acc = jnp.dot(lhs_scr[...], jnp.concatenate(blocks, axis=0), preferred_element_type=f32)
-    out_ref[0] = (gate_ref[0] * acc).astype(bf16)
-
-
-def out_rows(place, gate, pieces, own_w, near_w, far_w, sample, samples, previous):
-    hops = len(pieces)
-    block, cols = pieces[0].shape[1:]
+        cols = pieces[0].shape[2]
+        half = cols // 2
+        for sample in range(samples):
+            span = slice(sample * block, (sample + 1) * block)
+            lhs_scr[span, :cols] = pieces[sample * hops][0]
+            for hop in range(1, hops):
+                rows = pieces[sample * hops + hop][0]
+                low, high = rows[:, :half].astype(f32), rows[:, half:].astype(f32)
+                at = hop * cols
+                lhs_scr[span, at : at + half] = jnp.where(first, low, high).astype(bf16)
+                lhs_scr[span, at + half : at + cols] = jnp.where(first, high, low).astype(bf16)
+
+    joined = jnp.concatenate([weight[...] for weight in weights], axis=0)
+    acc = jnp.dot(lhs_scr[...], joined, preferred_element_type=f32)
+    for sample in range(samples):
+        out_ref[sample] = (gate_ref[sample] * acc[sample * block : (sample + 1) * block]).astype(bf16)
+
+
+def out_rows(place, gate, arrived, own_w, near_w, far_w):
+    samples, hops = len(arrived), len(arrived[0])
+    block, cols = arrived[0][0].shape[1:]
     width = own_w.shape[1]
     tile = min(512, width)
-    specs = [pl.BlockSpec((1, 1, tile), lambda n, *_: (sample, 0, n))]
-    specs += [pl.BlockSpec((1, block, cols), lambda n, *_: (0, 0, 0))] * hops
-    specs += [pl.BlockSpec((cols, tile), lambda n, *_: (0, n))]
-    specs += [pl.BlockSpec((cols // 2, tile), lambda n, *_: (0, n))] * (2 * (hops - 1))
-    args = [gate, *pieces, own_w, *near_w, *far_w]
-    aliases = {}
-    if previous is not None:
-        specs.append(pl.BlockSpec(memory_space=pl.ANY))
-        args.append(previous)
-        aliases = {len(args): 0}
+    weights = [own_w]
+    for near, far in zip(near_w, far_w):
+        weights += [near, far]
+    pieces = [piece for group in arrived for piece in group]
+    specs = [pl.BlockSpec((gate.shape[0], 1, tile), lambda n, *_: (0, 0, n))]
+    specs += [pl.BlockSpec((1, block, cols), lambda n, *_: (0, 0, 0))] * len(pieces)
+    specs += [pl.BlockSpec((weight.shape[0], tile), lambda n, *_: (0, n)) for weight in weights]
+    depth = hops * cols
     return pl.pallas_call(
-        functools.partial(out_kernel, hops=hops),
+        functools.partial(out_kernel, hops=hops, samples=samples),
         grid_spec=pltpu.PrefetchScalarGridSpec(
             num_scalar_prefetch=1,
             grid=(width // tile,),
             in_specs=specs,
-            out_specs=pl.BlockSpec((1, block, tile), lambda n, *_: (sample, 0, n)),
-            scratch_shapes=[pltpu.VMEM((block, hops * cols), bf16)],
+            out_specs=pl.BlockSpec((samples, block, tile), lambda n, *_: (0, 0, n)),
+            scratch_shapes=[pltpu.VMEM((samples * block, depth), bf16)],
         ),
         out_shape=jax.ShapeDtypeStruct((samples, block, width), bf16),
-        input_output_aliases=aliases,
         cost_estimate=pl.CostEstimate(
-            flops=2 * block * hops * cols * width, transcendentals=0, bytes_accessed=2 * hops * cols * width
+            flops=2 * samples * block * depth * width, transcendentals=0, bytes_accessed=2 * depth * width
         ),
         name="out_proj",
-    )(place, *args)
+    )(place, gate, *pieces, *weights)
 
 
 def shards(
@@ -468,10 +464,7 @@
         arrived.append(
             [attended[:1]] + [shifted(attended[hop : hop + 1], "tp", hop) for hop in range(1, tp_count)]
         )
-    mixed = None
-    for sample in range(samples):
-        mixed = out_rows(place, gate, arrived[sample], w_out, near_w, far_w, sample, samples, mixed)
-    return mixed
+    return out_rows(place, gate, arrived, w_out, near_w, far_w)
 
 
 def solution(mesh):

time: 110 us -> 114 us (1.036)
  waiting for transfers between devices: 9.42 us -> 20.4 us
  Pallas kernels: 59 us -> 54.3 us
  local copies, waits for them, and re-layouts: 12.7 us -> 10.7 us
    ppermute x21, waiting for transfers between devices: 9.42 us -> 20.4 us  [shifted(): lax.ppermute(piece, axis, [(i, (i + hop) % count) for i in range(count)])]
    pallas_call x2 -> x1, Pallas kernels: 11.9 us -> 7.17 us  [out_rows(): pl.pallas_call(functools.partial(out_kernel, hops=hops, samples=samples),...]
    unnamed x46 -> x42, local copies, waits for them, and re-layouts: 7.51 us -> 5.83 us
  transfers between devices with their start and end apart: 21 -> 21, of which waited for: 5 -> 7; matrix products, arithmetic and copies ran while one was open for 7% -> 7% of each run, Pallas kernels for 39% -> 33%
where the time goes in v3:
time: 114 us
  Pallas kernels  54.3 us (48%)
  starting transfers between devices  26.3 us (23%)
  waiting for transfers between devices  20.4 us (18%)
  local copies, waits for them, and re-layouts  10.7 us (9%)
  other arithmetic  1.71 us (2%)
    ppermute x21, starting transfers between devices, shifted(): lax.ppermute(piece, axis, [(i, (i + hop) % count) for i in range(count)])  26.3 us
    pallas_call x2, Pallas kernels, attended_rows(): pl.pallas_call(functools.partial(attend_kernel, pieces=pieces, last_place...  24.5 us
    ppermute x21, waiting for transfers between devices, shifted(): lax.ppermute(piece, axis, [(i, (i + hop) % count) for i in range(count)])  20.4 us
    pallas_call x1, Pallas kernels, projected_rows(): pl.pallas_call(proj_kernel, grid=(samples, tokens // block), in_specs=[pl...  12.7 us
    pallas_call x1, Pallas kernels, out_rows(): pl.pallas_call(functools.partial(out_kernel, hops=hops, samples=samples),...  7.17 us
    pallas_call x1, Pallas kernels, early_pairs(): pl.pallas_call(early_kernel, grid=(samples,), in_specs=[pl.BlockSpec((1,...  5.91 us
    unnamed x42, local copies, waits for them, and re-layouts  5.83 us
    slice x2, local copies, waits for them, and re-layouts, shards(): attended[hop:hop + 1]  3.53 us
  transfers between devices with their start and end apart: 21, of which 7 were waited for; matrix products, arithmetic and copies ran while one was open for 7% of the time, Pallas kernels for 33%

profile of v3, /device:TPU:0, one launch (start us, length us, event | category | flops | bytes accessed | tf_op | source)
XLA Modules:
  0.0 113.6 jit_solution(12242874088653883310)
XLA Ops:
  0.0 1.3 %broadcast_in_dim.22.ctx_ref = bf16[1,512]{1,0:T(2,128)(2,1)} reshape(bf16[512]{0:T(512)(128)(2,1)} %param.17) | data formatting | bytes 2048 | tf_op jit(solution)/shard_map/broadcast_in_dim | solution.py:71
  1.3 2.3 %mod_part.1 = f32[3,1536]{1,0:T(4,128)} custom-call(bf16[2,512]{1,0:T(2,128)(2,1)} %cond_ref.1, bf16[1,512]{1,0:T(2,128)(2,1)} %broadcast_in_dim.22.ctx_ref, bf16[512,512]{1,0:T(8,128)(2,1)} %shift_ref.1, bf16[512,512]{1,0:T(8,128)(2,1)} %scale_ref.1, bf16[512,512]{1,0:T(8,128)(2,1)} %gate_ref.1), custom_call_target="tpu_custom_call" | custom-call | tf_op jit(solution)/shard_map/mod_part/pallas_call | solution.py:66
  3.6 3.9 %collective-permute-start.2 = (f32[3,1536]{1,0:T(4,128)}, f32[3,1536]{1,0:T(4,128)S(1)}, u32[]{:S(2)}, u32[]{:S(2)}) collective-permute-start(f32[3,1536]{1,0:T(4,128)} %mod_part.1), channel_id=1, source_target_pairs={{0,6},{2,0},{4,2},{6,4},{1,7},{3,1},{5,3},{7,5},{8,14},{10,8},{12,... | collective-permute-start | bytes 55304 | tf_op jit(solution)/shard_map/ppermute | solution.py:27
  8.8 2.0 %copy.15.wk_ref = bf16[2048,64]{1,0:T(8,128)(2,1)} copy(bf16[2048,64]{0,1:T(8,128)(2,1)} %param.23) | data formatting | bytes 524288 | tf_op args[9]
  13.8 3.7 %collective-permute-start.5 = (f32[4,3,1536]{2,1,0:T(4,128)S(1)}, f32[4,3,1536]{2,1,0:T(4,128)S(1)}, u32[]{:S(2)}, u32[]{:S(2)}) collective-permute-start(f32[4,3,1536]{2,1,0:T(4,128)S(1)} %pad_maximum_fusion.refs_0_), channel_id=1, source_target_pairs={{0,24},{8,0},{16,8},{24,16},{1,25},{9,1},{17,9},{25,17},{2,26},{10... | collective-permute-start | bytes 221192 | tf_op jit(solution)/shard_map/ppermute | solution.py:27
  20.0 5.1 %collective-permute-done.4.refs_2_ = f32[4,3,1536]{2,1,0:T(4,128)S(1)} collective-permute-done((f32[4,3,1536]{2,1,0:T(4,128)S(1)}, f32[4,3,1536]{2,1,0:T(4,128)S(1)}, u32[]{:S(2)}, u32[]{:S(2)}) %collective-permute-start.4) | collective-permute-done | bytes 73760 | tf_op jit(solution)/shard_map/ppermute | solution.py:27
  25.7 1.7 %finish.1 = (f32[3,1,2048]{2,1,0:T(1,128)}, f32[3,1,2048]{2,1,0:T(1,128)}, f32[3,1,2048]{2,1,0:T(1,128)}) custom-call(s32[3]{0:T(128)} %copy-done.6, f32[1,2048]{1,0:T(1,128)} %bitcast.14, f32[4,3,1536]{2,1,0:T(4,128)} %copy-done, f32[4,3,1536]{2,1,0:T(4,128)} %copy-done.5, f32[4,3,1536]{2,1,0:T(4,128)} %copy-done.4, f32[4,3,1536]{2,1,0:T(4,128)} %copy-done.3), custom_call_target="tpu_custom_call" | custom-call | tf_op jit(solution)/shard_map/finish/pallas_call | solution.py:83
  27.4 5.9 %early_proj.1 = (bf16[2,256,128]{2,1,0:T(8,128)(2,1)}, bf16[2,384,128]{2,1,0:T(8,128)(2,1)}, bf16[2,384,128]{2,1,0:T(8,128)(2,1)}) custom-call(bf16[2,256,2048]{2,1,0:T(8,128)(2,1)} %x_ref.3, bf16[2,1024,2048]{2,1,0:T(8,128)(2,1)} %tail_ref.1, bf16[2,1024,2048]{2,1,0:T(8,128)(2,1)} %tail_ref.1, f32[3,1,2048]{2,1,0:T(1,128)} %get-tuple-element.16.gain_ref.cgain_ref, ...), custom_call_target="tpu_custom_call" | custom-call | flops 536870912 | bytes 4194304 | tf_op jit(solution)/shard_map/early_proj/pallas_call | solution.py:171
  33.3 1.7 %collective-permute-start.8 = (bf16[2,256,128]{2,1,0:T(8,128)(2,1)}, bf16[2,256,128]{2,1,0:T(8,128)(2,1)S(1)}, u32[]{:S(2)}, u32[]{:S(2)}) collective-permute-start(bf16[2,256,128]{2,1,0:T(8,128)(2,1)} %get-tuple-element.23.rest_0_), channel_id=1, source_target_pairs={{0,16},{8,24},{16,0},{24,8},{1,17},{9,25},{17,1},{25,9},{2,18},{10... | collective-permute-start | bytes 393224 | tf_op jit(solution)/shard_map/ppermute | solution.py:27
  35.1 2.0 %collective-permute-start.19 = (bf16[128,2048]{1,0:T(8,128)(2,1)S(1)}, bf16[128,2048]{1,0:T(8,128)(2,1)S(1)}, u32[]{:S(2)}, u32[]{:S(2)}) collective-permute-start(bf16[128,2048]{1,0:T(8,128)(2,1)S(1)} %constant_dynamic-slice_fusion), channel_id=1, source_target_pairs={{0,6},{2,0},{4,2},{6,4},{1,7},{3,1},{5,3},{7,5},{8,14},{10,8},{12,... | collective-permute-start | bytes 1572872 | tf_op jit(solution)/shard_map/ppermute | solution.py:27
  37.2 1.5 %collective-permute-start.17 = (bf16[128,2048]{1,0:T(8,128)(2,1)S(1)}, bf16[128,2048]{1,0:T(8,128)(2,1)S(1)}, u32[]{:S(2)}, u32[]{:S(2)}) collective-permute-start(bf16[128,2048]{1,0:T(8,128)(2,1)S(1)} %constant_dynamic-slice_fusion), channel_id=1, source_target_pairs={{0,4},{2,6},{4,0},{6,2},{1,5},{3,7},{5,1},{7,3},{8,12},{10,14},{12... | collective-permute-start | bytes 1572872 | tf_op jit(solution)/shard_map/ppermute | solution.py:27
  39.2 1.9 %collective-permute-done.8.rest_3_ = bf16[2,256,128]{2,1,0:T(8,128)(2,1)S(1)} collective-permute-done((bf16[2,256,128]{2,1,0:T(8,128)(2,1)}, bf16[2,256,128]{2,1,0:T(8,128)(2,1)S(1)}, u32[]{:S(2)}, u32[]{:S(2)}) %collective-permute-start.8) | collective-permute-done | bytes 131104 | tf_op jit(solution)/shard_map/ppermute | solution.py:27
  41.0 2.9 %collective-permute-start.7 = (bf16[2,384,128]{2,1,0:T(8,128)(2,1)}, bf16[2,384,128]{2,1,0:T(8,128)(2,1)S(1)}, u32[]{:S(2)}, u32[]{:S(2)}) collective-permute-start(bf16[2,384,128]{2,1,0:T(8,128)(2,1)} %get-tuple-element.22), channel_id=1, source_target_pairs={{0,24},{8,0},{16,8},{24,16},{1,25},{9,1},{17,9},{25,17},{2,26},{10... | collective-permute-start | bytes 589832 | tf_op jit(solution)/shard_map/ppermute | solution.py:27
  43.9 12.7 %latent_proj.1 = (bf16[2,1024,256]{2,1,0:T(8,128)(2,1)}, bf16[2,1024,128]{2,1,0:T(8,128)(2,1)}) custom-call(bf16[2,1024,2048]{2,1,0:T(8,128)(2,1)} %tail_ref.1, f32[3,1,2048]{2,1,0:T(1,128)} %get-tuple-element.16.gain_ref.cgain_ref, f32[3,1,2048]{2,1,0:T(1,128)} %get-tuple-element.17.shift_ref.cshift_ref, bf16[2048,256]{1,0:T(8,128)(2,1)} %wq_ref.1, ...), custom_call_target="tpu_custom_call" | custom-call | flops 3221225472 | bytes 8388608 | tf_op jit(solution)/shard_map/latent_proj/pallas_call | solution.py:223
  57.4 12.2 %attend.3 = bf16[4,256,256]{2,1,0:T(8,128)(2,1)} custom-call(s32[3]{0:T(128)} %copy-done.6, f32[4]{0:T(128)} %lift_ref.3, f32[4]{0:T(128)} %sink_ref.3, bf16[2,1024,256]{2,1,0:T(8,128)(2,1)} %get-tuple-element.19.q_ref, bf16[2,1024,128]{2,1,0:T(8,128)(2,1)} %get-tuple-element.20.kv_ref, bf16[2,384,128]{2,1,0:T(8,128)(2,1)} %copy-done.13, ...), custom_call_target="tpu_custom_call" | custom-call | flops 1476395008 | bytes 360448 | tf_op jit(solution)/shard_map/attend/pallas_call | solution.py:349
  69.6 1.8 %fusion.7 = (bf16[1,256,256]{2,1,0:T(8,128)(2,1)S(1)}, bf16[1,256,256]{2,1,0:T(8,128)(2,1)S(1)}, bf16[1,256,256]{2,1,0:T(8,128)(2,1)S(1)}, bf16[1,256,256]{2,1,0:T(8,128)(2,1)}) fusion(bf16[4,256,256]{2,1,0:T(8,128)(2,1)} %attend.3), kind=kLoop, calls=%fused_computation.26 | loop fusion | bytes 1048576 | tf_op jit(solution)/shard_map/slice | solution.py:465
  71.4 1.8 %collective-permute-start.14 = (bf16[1,256,256]{2,1,0:T(8,128)(2,1)S(1)}, bf16[1,256,256]{2,1,0:T(8,128)(2,1)}, u32[]{:S(2)}, u32[]{:S(2)}) collective-permute-start(bf16[1,256,256]{2,1,0:T(8,128)(2,1)S(1)} %get-tuple-element.25), channel_id=1, source_target_pairs={{0,6},{2,0},{4,2},{6,4},{1,7},{3,1},{5,3},{7,5},{8,14},{10,8},{12,... | collective-permute-start | bytes 393224 | tf_op jit(solution)/shard_map/ppermute | solution.py:27
  73.2 2.1 %collective-permute-start.13 = (bf16[1,256,256]{2,1,0:T(8,128)(2,1)S(1)}, bf16[1,256,256]{2,1,0:T(8,128)(2,1)}, u32[]{:S(2)}, u32[]{:S(2)}) collective-permute-start(bf16[1,256,256]{2,1,0:T(8,128)(2,1)S(1)} %get-tuple-element.26), channel_id=1, source_target_pairs={{0,4},{2,6},{4,0},{6,2},{1,5},{3,7},{5,1},{7,3},{8,12},{10,14},{12... | collective-permute-start | bytes 393224 | tf_op jit(solution)/shard_map/ppermute | solution.py:27
  75.9 12.2 %attend.2 = bf16[4,256,256]{2,1,0:T(8,128)(2,1)} custom-call(s32[3]{0:T(128)} %copy-done.6, f32[4]{0:T(128)} %lift_ref.3, f32[4]{0:T(128)} %sink_ref.3, bf16[2,1024,256]{2,1,0:T(8,128)(2,1)} %get-tuple-element.19.q_ref, bf16[2,1024,128]{2,1,0:T(8,128)(2,1)} %get-tuple-element.20.kv_ref, bf16[2,384,128]{2,1,0:T(8,128)(2,1)} %copy-done.13, ...), custom_call_target="tpu_custom_call" | custom-call | flops 1476395008 | bytes 360448 | tf_op jit(solution)/shard_map/attend/pallas_call | solution.py:349
  88.1 1.8 %fusion.8 = (bf16[1,256,256]{2,1,0:T(8,128)(2,1)S(1)}, bf16[1,256,256]{2,1,0:T(8,128)(2,1)S(1)}, bf16[1,256,256]{2,1,0:T(8,128)(2,1)S(1)}, bf16[1,256,256]{2,1,0:T(8,128)(2,1)}) fusion(bf16[4,256,256]{2,1,0:T(8,128)(2,1)} %attend.2), kind=kLoop, calls=%fused_computation.27 | loop fusion | bytes 1048576 | tf_op jit(solution)/shard_map/slice | solution.py:465
  89.9 2.9 %collective-permute-start.11 = (bf16[1,256,256]{2,1,0:T(8,128)(2,1)S(1)}, bf16[1,256,256]{2,1,0:T(8,128)(2,1)S(1)}, u32[]{:S(2)}, u32[]{:S(2)}) collective-permute-start(bf16[1,256,256]{2,1,0:T(8,128)(2,1)S(1)} %get-tuple-element.29), channel_id=1, source_target_pairs={{0,6},{2,0},{4,2},{6,4},{1,7},{3,1},{5,3},{7,5},{8,14},{10,8},{12,... | collective-permute-start | bytes 393224 | tf_op jit(solution)/shard_map/ppermute | solution.py:27
  92.8 4.3 %collective-permute-done.12.refs_5_ = bf16[1,256,256]{2,1,0:T(8,128)(2,1)S(1)} collective-permute-done((bf16[1,256,256]{2,1,0:T(8,128)(2,1)S(1)}, bf16[1,256,256]{2,1,0:T(8,128)(2,1)S(1)}, u32[]{:S(2)}, u32[]{:S(2)}) %collective-permute-start.12) | collective-permute-done | bytes 131104 | tf_op jit(solution)/shard_map/ppermute | solution.py:27
  98.6 6.4 %collective-permute-done.10.refs_2_ = bf16[1,256,256]{2,1,0:T(8,128)(2,1)S(1)} collective-permute-done((bf16[1,256,256]{2,1,0:T(8,128)(2,1)S(1)}, bf16[1,256,256]{2,1,0:T(8,128)(2,1)S(1)}, u32[]{:S(2)}, u32[]{:S(2)}) %collective-permute-start.10) | collective-permute-done | bytes 131104 | tf_op jit(solution)/shard_map/ppermute | solution.py:27
  106.4 7.2 %out_proj.1 = bf16[2,256,2048]{2,1,0:T(8,128)(2,1)} custom-call(s32[3]{0:T(128)} %copy-done.6, f32[3,1,2048]{2,1,0:T(1,128)} %get-tuple-element.15.gate_ref, bf16[1,256,256]{2,1,0:T(8,128)(2,1)} %get-tuple-element.32.refs_0_, bf16[1,256,256]{2,1,0:T(8,128)(2,1)} %copy-done.19, bf16[1,256,256]{2,1,0:T(8,128)(2,1)} %copy-done.18, ...), custom_call_target="tpu_custom_call" | custom-call | flops 2147483648 | bytes 4194304 | tf_op jit(solution)/shard_map/out_proj/pallas_call | solution.py:398
  (78 shorter events, 12.0 us)
Async XLA Ops:
  3.6 8.1 %collective-permute-start.2 = (f32[3,1536]{1,0:T(4,128)}, f32[3,1536]{1,0:T(4,128)S(1)}, u32[]{:S(2)}, u32[]{:S(2)}) collective-permute-start(f32[3,1536]{1,0:T(4,128)} %mod_part.1), channel_id=1, source_target_pairs={{0,6},{2,0},{4,2},{6,4},{1,7},{3,1},{5,3},{7,5},{8,14},{10,8},{12,... | collective-permute-start | bytes 55304 | tf_op jit(solution)/shard_map/ppermute | solution.py:27
  7.5 4.2 %collective-permute-start.1 = (f32[3,1536]{1,0:T(4,128)}, f32[3,1536]{1,0:T(4,128)S(1)}, u32[]{:S(2)}, u32[]{:S(2)}) collective-permute-start(f32[3,1536]{1,0:T(4,128)} %mod_part.1), channel_id=1, source_target_pairs={{0,4},{2,6},{4,0},{6,2},{1,5},{3,7},{5,1},{7,3},{8,12},{10,14},{12... | collective-permute-start | bytes 55304 | tf_op jit(solution)/shard_map/ppermute | solution.py:27
  8.1 4.9 %collective-permute-start = (f32[3,1536]{1,0:T(4,128)}, f32[3,1536]{1,0:T(4,128)S(1)}, u32[]{:S(2)}, u32[]{:S(2)}) collective-permute-start(f32[3,1536]{1,0:T(4,128)} %mod_part.1), channel_id=1, source_target_pairs={{0,2},{2,4},{4,6},{6,0},{1,3},{3,5},{5,7},{7,1},{8,10},{10,12},{12... | collective-permute-start | bytes 55304 | tf_op jit(solution)/shard_map/ppermute | solution.py:27
  8.8 16.3 %copy-start.6 = (s32[3]{0:T(128)}, s32[3]{0:T(128)S(1)}, u32[]{:S(2)}) copy-start(s32[3]{0:T(128)S(1)} %pad_add_fusion.place_ref) | copy-start | bytes 40
  13.8 6.1 %collective-permute-start.5 = (f32[4,3,1536]{2,1,0:T(4,128)S(1)}, f32[4,3,1536]{2,1,0:T(4,128)S(1)}, u32[]{:S(2)}, u32[]{:S(2)}) collective-permute-start(f32[4,3,1536]{2,1,0:T(4,128)S(1)} %pad_maximum_fusion.refs_0_), channel_id=1, source_target_pairs={{0,24},{8,0},{16,8},{24,16},{1,25},{9,1},{17,9},{25,17},{2,26},{10... | collective-permute-start | bytes 221192 | tf_op jit(solution)/shard_map/ppermute | solution.py:27
  17.5 7.6 %collective-permute-start.4 = (f32[4,3,1536]{2,1,0:T(4,128)S(1)}, f32[4,3,1536]{2,1,0:T(4,128)S(1)}, u32[]{:S(2)}, u32[]{:S(2)}) collective-permute-start(f32[4,3,1536]{2,1,0:T(4,128)S(1)} %pad_maximum_fusion.refs_0_), channel_id=1, source_target_pairs={{0,16},{8,24},{16,0},{24,8},{1,17},{9,25},{17,1},{25,9},{2,18},{10... | collective-permute-start | bytes 221192 | tf_op jit(solution)/shard_map/ppermute | solution.py:27
  17.5 7.6 %collective-permute-start.3 = (f32[4,3,1536]{2,1,0:T(4,128)S(1)}, f32[4,3,1536]{2,1,0:T(4,128)S(1)}, u32[]{:S(2)}, u32[]{:S(2)}) collective-permute-start(f32[4,3,1536]{2,1,0:T(4,128)S(1)} %pad_maximum_fusion.refs_0_), channel_id=1, source_target_pairs={{0,8},{8,16},{16,24},{24,0},{1,9},{9,17},{17,25},{25,1},{2,10},{10... | collective-permute-start | bytes 221192 | tf_op jit(solution)/shard_map/ppermute | solution.py:27
  33.3 7.7 %collective-permute-start.8 = (bf16[2,256,128]{2,1,0:T(8,128)(2,1)}, bf16[2,256,128]{2,1,0:T(8,128)(2,1)S(1)}, u32[]{:S(2)}, u32[]{:S(2)}) collective-permute-start(bf16[2,256,128]{2,1,0:T(8,128)(2,1)} %get-tuple-element.23.rest_0_), channel_id=1, source_target_pairs={{0,16},{8,24},{16,0},{24,8},{1,17},{9,25},{17,1},{25,9},{2,18},{10... | collective-permute-start | bytes 393224 | tf_op jit(solution)/shard_map/ppermute | solution.py:27
  35.1 40.1 %collective-permute-start.19 = (bf16[128,2048]{1,0:T(8,128)(2,1)S(1)}, bf16[128,2048]{1,0:T(8,128)(2,1)S(1)}, u32[]{:S(2)}, u32[]{:S(2)}) collective-permute-start(bf16[128,2048]{1,0:T(8,128)(2,1)S(1)} %constant_dynamic-slice_fusion), channel_id=1, source_target_pairs={{0,6},{2,0},{4,2},{6,4},{1,7},{3,1},{5,3},{7,5},{8,14},{10,8},{12,... | collective-permute-start | bytes 1572872 | tf_op jit(solution)/shard_map/ppermute | solution.py:27
  37.2 38.1 %collective-permute-start.17 = (bf16[128,2048]{1,0:T(8,128)(2,1)S(1)}, bf16[128,2048]{1,0:T(8,128)(2,1)S(1)}, u32[]{:S(2)}, u32[]{:S(2)}) collective-permute-start(bf16[128,2048]{1,0:T(8,128)(2,1)S(1)} %constant_dynamic-slice_fusion), channel_id=1, source_target_pairs={{0,4},{2,6},{4,0},{6,2},{1,5},{3,7},{5,1},{7,3},{8,12},{10,14},{12... | collective-permute-start | bytes 1572872 | tf_op jit(solution)/shard_map/ppermute | solution.py:27
  38.7 37.1 %collective-permute-start.15 = (bf16[128,2048]{1,0:T(8,128)(2,1)S(1)}, bf16[128,2048]{1,0:T(8,128)(2,1)S(1)}, u32[]{:S(2)}, u32[]{:S(2)}) collective-permute-start(bf16[128,2048]{1,0:T(8,128)(2,1)S(1)} %constant_dynamic-slice_fusion), channel_id=1, source_target_pairs={{0,2},{2,4},{4,6},{6,0},{1,3},{3,5},{5,7},{7,1},{8,10},{10,12},{12... | collective-permute-start | bytes 1572872 | tf_op jit(solution)/shard_map/ppermute | solution.py:27
  38.7 17.9 %collective-permute-start.6 = (bf16[2,384,128]{2,1,0:T(8,128)(2,1)}, bf16[2,384,128]{2,1,0:T(8,128)(2,1)S(1)}, u32[]{:S(2)}, u32[]{:S(2)}) collective-permute-start(bf16[2,384,128]{2,1,0:T(8,128)(2,1)} %get-tuple-element.21), channel_id=1, source_target_pairs={{0,8},{8,16},{16,24},{24,0},{1,9},{9,17},{17,25},{25,1},{2,10},{10... | collective-permute-start | bytes 589832 | tf_op jit(solution)/shard_map/ppermute | solution.py:27
  41.0 15.6 %copy-start.15 = (bf16[2,256,128]{2,1,0:T(8,128)(2,1)}, bf16[2,256,128]{2,1,0:T(8,128)(2,1)S(1)}, u32[]{:S(2)}) copy-start(bf16[2,256,128]{2,1,0:T(8,128)(2,1)S(1)} %collective-permute-done.8.rest_3_) | copy-start | bytes 393220
  41.0 15.6 %collective-permute-start.7 = (bf16[2,384,128]{2,1,0:T(8,128)(2,1)}, bf16[2,384,128]{2,1,0:T(8,128)(2,1)S(1)}, u32[]{:S(2)}, u32[]{:S(2)}) collective-permute-start(bf16[2,384,128]{2,1,0:T(8,128)(2,1)} %get-tuple-element.22), channel_id=1, source_target_pairs={{0,24},{8,0},{16,8},{24,16},{1,25},{9,1},{17,9},{25,17},{2,26},{10... | collective-permute-start | bytes 589832 | tf_op jit(solution)/shard_map/ppermute | solution.py:27
  71.4 18.5 %collective-permute-start.14 = (bf16[1,256,256]{2,1,0:T(8,128)(2,1)S(1)}, bf16[1,256,256]{2,1,0:T(8,128)(2,1)}, u32[]{:S(2)}, u32[]{:S(2)}) collective-permute-start(bf16[1,256,256]{2,1,0:T(8,128)(2,1)S(1)} %get-tuple-element.25), channel_id=1, source_target_pairs={{0,6},{2,0},{4,2},{6,4},{1,7},{3,1},{5,3},{7,5},{8,14},{10,8},{12,... | collective-permute-start | bytes 393224 | tf_op jit(solution)/shard_map/ppermute | solution.py:27
  73.2 16.7 %collective-permute-start.13 = (bf16[1,256,256]{2,1,0:T(8,128)(2,1)S(1)}, bf16[1,256,256]{2,1,0:T(8,128)(2,1)}, u32[]{:S(2)}, u32[]{:S(2)}) collective-permute-start(bf16[1,256,256]{2,1,0:T(8,128)(2,1)S(1)} %get-tuple-element.26), channel_id=1, source_target_pairs={{0,4},{2,6},{4,0},{6,2},{1,5},{3,7},{5,1},{7,3},{8,12},{10,14},{12... | collective-permute-start | bytes 393224 | tf_op jit(solution)/shard_map/ppermute | solution.py:27
  75.3 12.9 %copy-start.7 = (bf16[128,2048]{1,0:T(8,128)(2,1)}, bf16[128,2048]{1,0:T(8,128)(2,1)S(1)}, u32[]{:S(2)}) copy-start(bf16[128,2048]{1,0:T(8,128)(2,1)S(1)} %collective-permute-done.19.refs_13_) | copy-start | bytes 1572868
  75.3 29.7 %collective-permute-start.20 = (bf16[128,2048]{1,0:T(8,128)(2,1)S(1)}, bf16[128,2048]{1,0:T(8,128)(2,1)S(1)}, u32[]{:S(2)}, u32[]{:S(2)}) collective-permute-start(bf16[128,2048]{1,0:T(8,128)(2,1)S(1)} %collective-permute-done.19.refs_13_), channel_id=1, source_target_pairs={{0,1},{1,0},{2,3},{3,2},{4,5},{5,4},{6,7},{7,6},{8,9},{9,8},{10,11... | collective-permute-start | bytes 1572872 | tf_op jit(solution)/shard_map/ppermute | solution.py:27
  75.3 29.7 %collective-permute-start.18 = (bf16[128,2048]{1,0:T(8,128)(2,1)S(1)}, bf16[128,2048]{1,0:T(8,128)(2,1)S(1)}, u32[]{:S(2)}, u32[]{:S(2)}) collective-permute-start(bf16[128,2048]{1,0:T(8,128)(2,1)S(1)} %collective-permute-done.17.refs_11_), channel_id=1, source_target_pairs={{0,1},{1,0},{2,3},{3,2},{4,5},{5,4},{6,7},{7,6},{8,9},{9,8},{10,11... | collective-permute-start | bytes 1572872 | tf_op jit(solution)/shard_map/ppermute | solution.py:27
  75.8 29.2 %collective-permute-start.16 = (bf16[128,2048]{1,0:T(8,128)(2,1)S(1)}, bf16[128,2048]{1,0:T(8,128)(2,1)S(1)}, u32[]{:S(2)}, u32[]{:S(2)}) collective-permute-start(bf16[128,2048]{1,0:T(8,128)(2,1)S(1)} %collective-permute-done.15.refs_9_), channel_id=1, source_target_pairs={{0,1},{1,0},{2,3},{3,2},{4,5},{5,4},{6,7},{7,6},{8,9},{9,8},{10,11... | collective-permute-start | bytes 1572872 | tf_op jit(solution)/shard_map/ppermute | solution.py:27
  89.9 7.3 %collective-permute-start.12 = (bf16[1,256,256]{2,1,0:T(8,128)(2,1)S(1)}, bf16[1,256,256]{2,1,0:T(8,128)(2,1)S(1)}, u32[]{:S(2)}, u32[]{:S(2)}) collective-permute-start(bf16[1,256,256]{2,1,0:T(8,128)(2,1)S(1)} %get-tuple-element.27), channel_id=1, source_target_pairs={{0,2},{2,4},{4,6},{6,0},{1,3},{3,5},{5,7},{7,1},{8,10},{10,12},{12... | collective-permute-start | bytes 393224 | tf_op jit(solution)/shard_map/ppermute | solution.py:27
  89.9 8.1 %collective-permute-start.11 = (bf16[1,256,256]{2,1,0:T(8,128)(2,1)S(1)}, bf16[1,256,256]{2,1,0:T(8,128)(2,1)S(1)}, u32[]{:S(2)}, u32[]{:S(2)}) collective-permute-start(bf16[1,256,256]{2,1,0:T(8,128)(2,1)S(1)} %get-tuple-element.29), channel_id=1, source_target_pairs={{0,6},{2,0},{4,2},{6,4},{1,7},{3,1},{5,3},{7,5},{8,14},{10,8},{12,... | collective-permute-start | bytes 393224 | tf_op jit(solution)/shard_map/ppermute | solution.py:27
  97.2 7.8 %collective-permute-start.10 = (bf16[1,256,256]{2,1,0:T(8,128)(2,1)S(1)}, bf16[1,256,256]{2,1,0:T(8,128)(2,1)S(1)}, u32[]{:S(2)}, u32[]{:S(2)}) collective-permute-start(bf16[1,256,256]{2,1,0:T(8,128)(2,1)S(1)} %get-tuple-element.30), channel_id=1, source_target_pairs={{0,4},{2,6},{4,0},{6,2},{1,5},{3,7},{5,1},{7,3},{8,12},{10,14},{12... | collective-permute-start | bytes 393224 | tf_op jit(solution)/shard_map/ppermute | solution.py:27
  98.1 6.9 %collective-permute-start.9 = (bf16[1,256,256]{2,1,0:T(8,128)(2,1)S(1)}, bf16[1,256,256]{2,1,0:T(8,128)(2,1)S(1)}, u32[]{:S(2)}, u32[]{:S(2)}) collective-permute-start(bf16[1,256,256]{2,1,0:T(8,128)(2,1)S(1)} %get-tuple-element.31), channel_id=1, source_target_pairs={{0,2},{2,4},{4,6},{6,0},{1,3},{3,5},{5,7},{7,1},{8,10},{10,12},{12... | collective-permute-start | bytes 393224 | tf_op jit(solution)/shard_map/ppermute | solution.py:27
  (17 other events, 82.8 us)
